TPU v7x, 512 devices: a whole 4x8x8 slice. The times are simulated.
512 devices in a mesh: sp: 32 (over z, x), tp: 16 (over y, core).
Axes of the slice: x: 4, y: 8, z: 8, core: 2. Of those that a mesh axis runs over, the one named last changes fastest.
Arguments:
- conv_value: bfloat16 [8192, 1024], P('sp', 'tp'), may hold values from -15 to 15
- conv_gate: bfloat16 [8192, 1024], P('sp', 'tp'), may hold values from -8 to 8
- conv_taps: bfloat16 [31, 1024], P(None, 'tp'), may hold values from -1 to 1
- conv_gain: float32 [1024], P('tp'), may hold values from 0.1 to 1.9
- out_weight: bfloat16 [1024, 2048], P('tp'), may hold values from -0.1875 to 0.1875
- residual: bfloat16 [8192, 2048], P('sp'), may hold values from -6 to 6
- route_ids: int32 [8192, 2], P('sp'), may hold values from 0 to 31, all different within a row; in each aligned block of 256 rows (0 to 255, 256 to 511, ...) at most 32 rows name the same one
- route_weight: float32 [8192, 2], P('sp'), may hold values from 0.3 to 1.5
- expert_gate: bfloat16 [32, 2048, 4096], P('sp', None, 'tp'), may hold values from -0.125 to 0.125
- expert_up: bfloat16 [32, 2048, 4096], P('sp', None, 'tp'), may hold values from -0.125 to 0.125
- expert_down: bfloat16 [32, 4096, 2048], P('sp', 'tp'), may hold values from -0.09375 to 0.09375
Outputs:
- layer_out: bfloat16 [8192, 2048], P('sp', 'tp')
Inputs may be any that keep to these rules, and one draw needn't show every extreme that they name: `route_ids`: in each aligned block of 256 rows no expert is named by more than 32 rows; some expert is named by exactly 32 rows in some blocks.
All inputs are finite; a program needn't handle non-finite values.
Results may differ from a plain program's by a relative error of at most 0.017.
Values may be sent and summed in bfloat16 or wider, within the bound.
A program may use at most 64 MiB of HBM per device.

v0:
```python
import jax
import jax.numpy as jnp
from jax import lax
from jax.sharding import Mesh
from jax.sharding import PartitionSpec as P

TP = ("tp_0", "tp_1")


def passed_along(value, axis, steps):
    count = lax.axis_size(axis)
    initial, last = (max(0, -steps), min(count, count - steps))
    return lax.ppermute(value, axis, [(source, source + steps) for source in range(initial, last)])


def sent_to_all(value, axis):
    size = lax.axis_size(axis)
    return lax.all_to_all(
        jnp.broadcast_to(value[None], (size, *value.shape)), axis, 0, 0, tiled=True
    )


def over_copies(value, axis):
    everything = sent_to_all(value, axis)
    return jnp.sum(everything, axis=0)


def packed_total(arrays, axis):
    ends = [0]
    for a in arrays:
        ends.append(ends[-1] + a.size)
    so_far = over_copies(jnp.concatenate([a.ravel() for a in arrays]), axis)
    return tuple((so_far[b:e].reshape(a.shape) for a, b, e in zip(arrays, ends, ends[1:])))


def filled_up(lines, size):
    spare = -len(lines) % size
    return jnp.pad(lines, [(0, spare)] + [(0, 0)] * (lines.ndim - 1))


def laid_out(blocks, dim):
    blocks = jnp.moveaxis(blocks, 0, dim)
    shape = blocks.shape
    return blocks.reshape(*shape[:dim], shape[dim] * shape[dim + 1], *shape[dim + 2 :])


def gather_axes(value, axes, dim):
    far, near = axes
    initial = sent_to_all(value, far)
    blocks = jnp.swapaxes(sent_to_all(initial, near), 0, 1)
    return laid_out(blocks.reshape(-1, *value.shape), dim)


def split_up(value, dim, size):
    shape = value.shape
    blocks = value.reshape(*shape[:dim], size, shape[dim] // size, *shape[dim + 1 :])
    return jnp.moveaxis(blocks, dim, 0)


def summed_on_arrival(value, axis, dim):
    size = lax.axis_size(axis)
    blocks = lax.all_to_all(split_up(value, dim, size), axis, 0, 0, tiled=True)
    return jnp.sum(blocks.astype(jnp.float32), axis=0)


def sum_in_two_steps(value, axes, dim):
    far, near = axes
    blocks = split_up(value, dim, lax.axis_size(far))
    nearer = summed_on_arrival(blocks, near, dim + 1)
    arrived = lax.all_to_all(
        nearer.astype(jnp.bfloat16), far, split_axis=0, concat_axis=0, tiled=True
    )
    return arrived.astype(jnp.float32).sum(axis=0)


def sum_by_parts(value, axes):
    lines = value.reshape(-1, value.shape[-1])
    padded = filled_up(lines, lax.axis_size(axes[0]) * lax.axis_size(axes[1]))
    whole = gather_axes(sum_in_two_steps(padded, axes, 0).astype(jnp.bfloat16), axes, 0)
    return lax.slice_in_dim(whole, 0, len(lines)).reshape(value.shape).astype(jnp.float32)


def slot_plan(block_ids, experts, capacity):
    assigned = block_ids.reshape(-1)
    pair_count = assigned.shape[0]
    onehot = (assigned[:, None] == jnp.arange(experts, dtype=jnp.int32)[None, :]).astype(jnp.int32)
    earlier = jnp.cumsum(onehot, axis=0) - onehot
    ranking = jnp.sum(earlier * onehot, axis=1)
    target = assigned * capacity + ranking
    owners = jnp.arange(pair_count, dtype=jnp.int32) // block_ids.shape[1]
    matches = target[None, :] == jnp.arange(experts * capacity, dtype=jnp.int32)[:, None]
    holder = jnp.sum(jnp.where(matches, owners[None, :] + 1, 0), axis=1) - 1
    holder = jnp.where(holder < 0, block_ids.shape[0], holder)
    return (target, holder)


def local(
    conv_value,
    conv_gate,
    conv_taps,
    conv_gain,
    out_weight,
    residual,
    route_ids,
    route_weight,
    expert_gate,
    expert_up,
    expert_down,
):
    taps_count = conv_taps.shape[0]
    token_rows = conv_value.shape[0]
    tails = passed_along(
        (conv_value[token_rows - taps_count + 1 :], conv_gate[token_rows - taps_count + 1 :]),
        "sp",
        1,
    )
    values_ext = jnp.concatenate([tails[0], conv_value], axis=0)
    gates_ext = jnp.concatenate([tails[1], conv_gate], axis=0)
    gated = values_ext.astype(jnp.float32) * jax.nn.sigmoid(gates_ext.astype(jnp.float32))
    filtered = jnp.zeros(conv_value.shape, jnp.float32)
    for offset in range(taps_count):
        filtered = (
            filtered + conv_taps[offset].astype(jnp.float32) * gated[offset : offset + token_rows]
        )
    channels = conv_value.shape[1] * lax.axis_size(TP)
    totals = packed_total((jnp.sum(filtered, axis=1), jnp.sum(filtered * filtered, axis=1)), TP)
    average = totals[0] / channels
    variance = totals[1] / channels - average * average
    normed = (filtered - average[:, None]) * lax.rsqrt(variance + 1e-05)[:, None] * conv_gain
    activated = jax.nn.silu(normed).astype(jnp.bfloat16)
    mixed = sum_by_parts(
        jnp.dot(activated, out_weight, preferred_element_type=jnp.float32).astype(jnp.bfloat16),
        ("tp_0", "tp_1"),
    )
    updated = residual.astype(jnp.float32) + mixed
    width = updated.shape[1]
    normal_rows = (
        updated * lax.rsqrt(jnp.mean(updated * updated, axis=1, keepdims=True) + 1e-06)
    ).astype(jnp.bfloat16)
    experts = lax.axis_size("sp")
    top_count = route_ids.shape[1]
    capacity = 2 * token_rows * top_count // experts
    targets, holders = slot_plan(route_ids, experts, capacity)
    padded_rows = jnp.concatenate([normal_rows, jnp.zeros((1, width), jnp.bfloat16)], axis=0)
    buffer = padded_rows[holders].reshape(experts, capacity, width)
    w_gate = expert_gate[0]
    w_up = expert_up[0]
    w_down = expert_down[0]
    share = capacity // lax.axis_size(TP)
    mine = lax.dynamic_slice_in_dim(buffer, lax.axis_index(TP) * share, share, 1)
    arrived = lax.all_to_all(mine, "sp", split_axis=0, concat_axis=0, tiled=True)
    block = lax.all_gather(arrived, TP, axis=1, tiled=True)
    flat = block.reshape(-1, width)
    gate_act = jnp.dot(flat, w_gate, preferred_element_type=jnp.float32)
    up_act = jnp.dot(flat, w_up, preferred_element_type=jnp.float32)
    hidden = (jax.nn.silu(gate_act) * up_act).astype(jnp.bfloat16)
    result = jnp.dot(hidden, w_down, preferred_element_type=jnp.float32)
    partials = result.reshape(block.shape[0], block.shape[1], width)
    summed = sum_in_two_steps(partials.astype(jnp.bfloat16), ("tp_0", "tp_1"), 2).astype(
        jnp.bfloat16
    )
    back = lax.all_to_all(summed, "sp", split_axis=0, concat_axis=0, tiled=True)
    columns = back.shape[2]
    picked = back.reshape(experts * capacity, columns)[targets].reshape(
        token_rows, top_count, columns
    )
    combined = jnp.sum(picked.astype(jnp.float32) * route_weight[:, :, None], axis=1)
    own_cols = lax.dynamic_slice_in_dim(updated, lax.axis_index(TP) * columns, columns, 1)
    return (own_cols + combined).astype(jnp.bfloat16)


def solution(mesh):
    torus = Mesh(mesh.devices.reshape(mesh.shape["sp"], 8, 2), ("sp", "tp_0", "tp_1"))
    placed = (
        P("sp", TP),
        P("sp", TP),
        P(None, TP),
        P(TP),
        P(TP, None),
        P("sp", None),
        P("sp", None),
        P("sp", None),
        P("sp", None, TP),
        P("sp", None, TP),
        P("sp", TP, None),
    )
    return jax.shard_map(local, mesh=torus, in_specs=placed, out_specs=P("sp", TP), check_vma=False)
```

profile of v0, /device:TPU:1, one launch (start us, length us, event | category | flops | bytes accessed | tf_op | source)
XLA Modules:
  0.0 284.7 jit_solution(16322086723981687801)
XLA Ops:
  7.4 3.9 %collective-permute-start = (bf16[30,64]{0,1:T(8,128)(2,1)S(1)}, bf16[30,64]{0,1:T(8,128)(2,1)S(1)}, u32[]{:S(2)}, u32[]{:S(2)}) collective-permute-start(bf16[30,64]{0,1:T(8,128)(2,1)S(1)} %slice.205), channel_id=1, source_target_pairs={{0,16},{16,32},{32,48},{48,64},{64,80},{80,96},{96,112},{112,128},... | collective-permute-start | bytes 11528 | tf_op jit(solution)/shard_map/ppermute | solution.py:13
  12.2 3.1 %collective-permute-start.1 = (bf16[30,64]{0,1:T(8,128)(2,1)S(1)}, bf16[30,64]{0,1:T(8,128)(2,1)S(1)}, u32[]{:S(2)}, u32[]{:S(2)}) collective-permute-start(bf16[30,64]{0,1:T(8,128)(2,1)S(1)} %slice.206), channel_id=1, source_target_pairs={{0,16},{16,32},{32,48},{48,64},{64,80},{80,96},{96,112},{112,128},... | collective-permute-start | bytes 11528 | tf_op jit(solution)/shard_map/ppermute | solution.py:13
  19.1 15.5 %all_to_all.46 = f32[16,1,512]{2,1,0:T(1,128)S(1)} all-to-all(f32[16,1,512]{2,1,0:T(1,128)S(1)} %broadcast_in_dim.17), channel_id=1, replica_groups=mesh['sp'=32,'tp_0'=8,'tp_1'=2] {'tp_0','tp_1'}, dimensions={0} | all-to-all | bytes 65536 | tf_op jit(solution)/shard_map/all_to_all | solution.py:18
  35.3 4.6 %all_to_all.47 = bf16[2,8,16,2048]{3,2,1,0:T(8,128)(2,1)S(1)} all-to-all(bf16[2,8,16,2048]{3,2,1,0:T(8,128)(2,1)S(1)} %bitcast.163), channel_id=1, replica_groups=mesh['sp'=32,'tp_0'=8,'tp_1'=2] {'tp_1'}, dimensions={0} | all-to-all | bytes 2097152 | tf_op jit(solution)/shard_map/all_to_all | solution.py:62
  41.0 3.5 %all-to-all-start.2 = ((bf16[8,16,2048]{2,1,0:T(8,128)(2,1)}), bf16[8,16,2048]{2,1,0:T(8,128)(2,1)S(1)}, u32[]{:S(2)}, u32[]{:S(2)}) async-start(bf16[8,16,2048]{2,1,0:T(8,128)(2,1)} %reduce_sum.116), calls=%async_computation.2 | async-start | bytes 1048576 | tf_op jit(solution)/shard_map/all_to_all | solution.py:70
  46.5 15.9 %all-to-all-done.2 = bf16[8,16,2048]{2,1,0:T(8,128)(2,1)S(1)} async-done(((bf16[8,16,2048]{2,1,0:T(8,128)(2,1)}), bf16[8,16,2048]{2,1,0:T(8,128)(2,1)S(1)}, u32[]{:S(2)}, u32[]{:S(2)}) %all-to-all-start.2) | async-done | bytes 524320 | tf_op jit(solution)/shard_map/all_to_all | solution.py:70
  63.4 3.5 %all-to-all-start.3 = ((bf16[8,16,2048]{2,1,0:T(8,128)(2,1)}), bf16[8,16,2048]{2,1,0:T(8,128)(2,1)S(1)}, u32[]{:S(2)}, u32[]{:S(2)}) async-start(bf16[8,16,2048]{2,1,0:T(8,128)(2,1)} %broadcast_in_dim.18), calls=%async_computation.3 | async-start | bytes 1048576 | tf_op jit(solution)/shard_map/all_to_all | solution.py:18
  67.3 17.5 %all-to-all-done.3 = bf16[8,16,2048]{2,1,0:T(8,128)(2,1)S(1)} async-done(((bf16[8,16,2048]{2,1,0:T(8,128)(2,1)}), bf16[8,16,2048]{2,1,0:T(8,128)(2,1)S(1)}, u32[]{:S(2)}, u32[]{:S(2)}) %all-to-all-start.3) | async-done | bytes 524320 | tf_op jit(solution)/shard_map/all_to_all | solution.py:18
  84.8 4.7 %all_to_all.48 = bf16[2,8,16,2048]{3,2,1,0:T(8,128)(2,1)S(1)} all-to-all(bf16[2,8,16,2048]{3,2,1,0:T(8,128)(2,1)S(1)} %broadcast_in_dim.19), channel_id=1, replica_groups=mesh['sp'=32,'tp_0'=8,'tp_1'=2] {'tp_1'}, dimensions={0} | all-to-all | bytes 2097152 | tf_op jit(solution)/shard_map/all_to_all | solution.py:18
  91.4 1.4 copy-done.1
  93.1 6.0 %gather_fusion = bf16[1024,2048]{1,0:T(8,128)(2,1)} fusion(bf16[257,2048]{1,0:T(8,128)(2,1)S(1)} %concatenate.15, s32[1024]{0:T(1024)S(1)} %broadcast_clamp_fusion), kind=kCustom, calls=%fused_computation | custom fusion | bytes 8392704 | tf_op jit(solution)/shard_map/gather | solution.py:145
  99.1 1.5 constant_dynamic-slice_fusion
  100.6 25.3 %all_to_all.49 = bf16[32,2,2048]{2,1,0:T(2,128)(2,1)S(1)} all-to-all(bf16[32,2,2048]{2,1,0:T(2,128)(2,1)S(1)} %constant_dynamic-slice_fusion), channel_id=1, replica_groups=mesh['sp'=32,'tp_0'=8,'tp_1'=2] {'sp'}, dimensions={0} | all-to-all | bytes 524288 | tf_op jit(solution)/shard_map/all_to_all | solution.py:151
  126.7 36.6 %all-gather.2.cloned.1.call-done = bf16[32,32,2048]{2,0,1:T(8,128)(2,1)} async-done(((bf16[32,2,2048]{2,0,1:T(8,128)(2,1)}), bf16[32,32,2048]{2,0,1:T(8,128)(2,1)}) %all-gather.2.cloned.1.call-update) | async-done | bytes 4194320 | tf_op jit(solution)/shard_map/all_gather | solution.py:152
  163.4 4.5 %copy.72 = bf16[32,32,2048]{2,1,0:T(8,128)(2,1)S(1)} copy(bf16[32,32,2048]{2,0,1:T(8,128)(2,1)} %all-gather.2.cloned.1.call-done) | data formatting | bytes 8388608 | tf_op jit(solution)/shard_map/all_gather | solution.py:152
  171.7 2.5 copy.88
  174.3 6.9 %reshape.142 = bf16[8,32,32,2,128]{4,3,2,1,0:T(2,128)(2,1)} reshape(bf16[8,32,32,256]{3,2,1,0:T(8,128)(2,1)} %bitcast.156) | data formatting | bytes 8388608 | tf_op jit(solution)/shard_map/reshape | solution.py:56
  181.2 6.1 %copy.74 = bf16[2,8,32,32,128]{4,1,3,2,0:T(8,128)(2,1)S(1)} copy(bf16[2,8,32,32,128]{4,0,3,2,1:T(2,128)(2,1)} %bitcast.157) | data formatting | bytes 8388608 | tf_op jit(solution)/shard_map/transpose | solution.py:57
  187.3 8.1 %all_to_all.50 = bf16[2,8,32,32,128]{4,1,3,2,0:T(8,128)(2,1)} all-to-all(bf16[2,8,32,32,128]{4,1,3,2,0:T(8,128)(2,1)S(1)} %copy.74), channel_id=1, replica_groups=mesh['sp'=32,'tp_0'=8,'tp_1'=2] {'tp_1'}, dimensions={0} | all-to-all | bytes 8388608 | tf_op jit(solution)/shard_map/all_to_all | solution.py:62
  195.4 3.3 %reduce_sum.121 = bf16[8,32,32,128]{3,0,2,1:T(8,128)(2,1)S(1)} reduce(bf16[2,8,32,32,128]{4,1,3,2,0:T(8,128)(2,1)} %all_to_all.50, bf16[]{:T(256)} %constant.58.clone.1), dimensions={0}, to_apply=%region_10.11 | reduce | flops 1048576 | bytes 6291458 | tf_op jit(solution)/shard_map/reduce_sum | solution.py:63
  199.1 54.1 %all_to_all.51 = bf16[8,32,32,128]{3,2,1,0:T(8,128)(2,1)S(1)} all-to-all(bf16[8,32,32,128]{3,2,1,0:T(8,128)(2,1)S(1)} %copy.76), channel_id=1, replica_groups=mesh['sp'=32,'tp_0'=8,'tp_1'=2] {'tp_0'}, dimensions={0} | all-to-all | bytes 4194304 | tf_op jit(solution)/shard_map/all_to_all | solution.py:70
  254.2 9.9 %all-to-all-start.8 = ((bf16[32,32,128]{2,1,0:T(8,128)(2,1)}), bf16[32,32,128]{2,1,0:T(8,128)(2,1)S(1)}, u32[]{:S(2)}, u32[]{:S(2)}) async-start(bf16[32,32,128]{2,1,0:T(8,128)(2,1)} %reduce_sum.122), calls=%async_computation.8 | async-start | bytes 524288 | tf_op jit(solution)/shard_map/all_to_all | solution.py:162
  264.6 9.9 %all-to-all-done.8 = bf16[32,32,128]{2,1,0:T(8,128)(2,1)S(1)} async-done(((bf16[32,32,128]{2,1,0:T(8,128)(2,1)}), bf16[32,32,128]{2,1,0:T(8,128)(2,1)S(1)}, u32[]{:S(2)}, u32[]{:S(2)}) %all-to-all-start.8) | async-done | bytes 262176 | tf_op jit(solution)/shard_map/all_to_all | solution.py:162
  276.3 1.6 add_convert_fusion
  (71 shorter events, 20.9 us)
Async XLA Ops:
  6.5 163.9 %copy-start = (bf16[1,256,2048]{2,1,0:T(8,128)(2,1)S(1)}, bf16[1,256,2048]{2,1,0:T(8,128)(2,1)}, u32[]{:S(2)}) copy-start(bf16[1,256,2048]{2,1,0:T(8,128)(2,1)} %param.21) | copy-start | bytes 3145732
  6.5 28.1 %copy-start.6 = (f32[64]{0:T(128)S(1)}, f32[64]{0:T(128)}, u32[]{:S(2)}) copy-start(f32[64]{0:T(128)} %param.14) | copy-start | bytes 772
  6.5 28.1 %copy-start.3 = (bf16[64,2048]{1,0:T(8,128)(2,1)S(1)}, bf16[64,2048]{1,0:T(8,128)(2,1)}, u32[]{:S(2)}) copy-start(bf16[64,2048]{1,0:T(8,128)(2,1)} %param.15) | copy-start | bytes 786436
  7.4 9.8 %collective-permute-start = (bf16[30,64]{0,1:T(8,128)(2,1)S(1)}, bf16[30,64]{0,1:T(8,128)(2,1)S(1)}, u32[]{:S(2)}, u32[]{:S(2)}) collective-permute-start(bf16[30,64]{0,1:T(8,128)(2,1)S(1)} %slice.205), channel_id=1, source_target_pairs={{0,16},{16,32},{32,48},{48,64},{64,80},{80,96},{96,112},{112,128},... | collective-permute-start | bytes 11528 | tf_op jit(solution)/shard_map/ppermute | solution.py:13
  12.2 5.1 %collective-permute-start.1 = (bf16[30,64]{0,1:T(8,128)(2,1)S(1)}, bf16[30,64]{0,1:T(8,128)(2,1)S(1)}, u32[]{:S(2)}, u32[]{:S(2)}) collective-permute-start(bf16[30,64]{0,1:T(8,128)(2,1)S(1)} %slice.206), channel_id=1, source_target_pairs={{0,16},{16,32},{32,48},{48,64},{64,80},{80,96},{96,112},{112,128},... | collective-permute-start | bytes 11528 | tf_op jit(solution)/shard_map/ppermute | solution.py:13
  35.3 9.2 %copy-start.4 = (s32[256,2]{0,1:T(2,128)S(1)}, s32[256,2]{0,1:T(2,128)}, u32[]{:S(2)}) copy-start(s32[256,2]{0,1:T(2,128)} %param.17) | copy-start | bytes 6148
  41.0 21.4 %all-to-all-start.2 = ((bf16[8,16,2048]{2,1,0:T(8,128)(2,1)}), bf16[8,16,2048]{2,1,0:T(8,128)(2,1)S(1)}, u32[]{:S(2)}, u32[]{:S(2)}) async-start(bf16[8,16,2048]{2,1,0:T(8,128)(2,1)} %reduce_sum.116), calls=%async_computation.2 | async-start | bytes 1048576 | tf_op jit(solution)/shard_map/all_to_all | solution.py:70
  63.4 21.4 %all-to-all-start.3 = ((bf16[8,16,2048]{2,1,0:T(8,128)(2,1)}), bf16[8,16,2048]{2,1,0:T(8,128)(2,1)S(1)}, u32[]{:S(2)}, u32[]{:S(2)}) async-start(bf16[8,16,2048]{2,1,0:T(8,128)(2,1)} %broadcast_in_dim.18), calls=%async_computation.3 | async-start | bytes 1048576 | tf_op jit(solution)/shard_map/all_to_all | solution.py:18
  66.9 96.5 %all-gather.2.cloned.1.call-start = ((), (), s32[]{:S(2)}) async-start(), calls=%async_computation.9 | async-start | bytes 4456448 | tf_op jit(solution)/shard_map/all_gather | solution.py:152
  89.8 1.2 copy-start.2
  91.4 1.4 copy-start.1
  126.7 41.1 %copy-start.7 = (bf16[1,2048,256]{2,1,0:T(8,128)(2,1)S(1)}, bf16[1,2048,256]{2,1,0:T(8,128)(2,1)}, u32[]{:S(2)}) copy-start(bf16[1,2048,256]{2,1,0:T(8,128)(2,1)} %param.19) | copy-start | bytes 3145732
  167.9 1.3 copy-start.8
  253.2 11.3 %copy-start.5 = (f32[256,2]{0,1:T(2,128)S(1)}, f32[256,2]{0,1:T(2,128)}, u32[]{:S(2)}) copy-start(f32[256,2]{0,1:T(2,128)} %param.18) | copy-start | bytes 6148
  254.2 20.3 %all-to-all-start.8 = ((bf16[32,32,128]{2,1,0:T(8,128)(2,1)}), bf16[32,32,128]{2,1,0:T(8,128)(2,1)S(1)}, u32[]{:S(2)}, u32[]{:S(2)}) async-start(bf16[32,32,128]{2,1,0:T(8,128)(2,1)} %reduce_sum.122), calls=%async_computation.8 | async-start | bytes 524288 | tf_op jit(solution)/shard_map/all_to_all | solution.py:162
Sparse Core Ops, SparseCore 0:
  126.8 36.4 all-gather.1
where the time goes:
time: 287 us; the launch traced here: 285 us
  blocking collectives  112 us (39%)
  waiting for transfers between devices  79.9 us (28%)
  local copies, waits for them, and re-layouts  36.6 us (13%)
  starting transfers between devices  24 us (8%)
  between operations  13.8 us (5%)
  other arithmetic  13.7 us (5%)
  matrix products  4.37 us (2%)
    all_to_all x1, blocking collectives, sum_in_two_steps(): lax.all_to_all(nearer.astype(jnp.bfloat16), far, split_axis=0, concat_axi...  54.1 us
    all_gather x1, waiting for transfers between devices, local(): block = lax.all_gather(arrived, TP, axis=1, tiled=True)  36.6 us
    all_to_all x1, blocking collectives, local(): lax.all_to_all(mine, 'sp', split_axis=0, concat_axis=0, tiled=True)  25.3 us
    all_to_all x2, blocking collectives, sent_to_all(): lax.all_to_all(jnp.broadcast_to(value[None], (size, *value.shape)), axis,...  20.2 us
    all_to_all x1, waiting for transfers between devices, sent_to_all(): lax.all_to_all(jnp.broadcast_to(value[None], (size, *value.shape)), axis,...  17.5 us
    all_to_all x1, waiting for transfers between devices, sum_in_two_steps(): lax.all_to_all(nearer.astype(jnp.bfloat16), far, split_axis=0, concat_axi...  15.9 us
    all_to_all x2, blocking collectives, summed_on_arrival(): blocks = lax.all_to_all(split_up(value, dim, size), axis, 0, 0, tiled=True)  12.7 us
    all_to_all x1, waiting for transfers between devices, local(): back = lax.all_to_all(summed, 'sp', split_axis=0, concat_axis=0, tiled=True)  9.92 us
  transfers between devices with their start and end apart: 6, of which 4 were waited for; matrix products, arithmetic and copies ran while one was open for 2% of the time, Pallas kernels for 0%

commit v1 on v0

v1 whole, which is shorter than its diff:
```python
import functools

import jax
import jax.numpy as jnp
from jax import lax
from jax.experimental import pallas as pl
from jax.experimental.pallas import tpu as pltpu
from jax.sharding import PartitionSpec as P

MESH = pl.DeviceIdType.MESH
F32, BF16 = jnp.float32, jnp.bfloat16
HALO = 32
ORDER = (0, 4, 1, 5, 2, 6, 3, 7)


def iota(shape, dim):
    return lax.broadcasted_iota(jnp.int32, shape, dim)


def matmul(a, b, precision=None):
    return jnp.dot(a, b, preferred_element_type=F32, precision=precision)


def layer(
    n_sp, n_y,
    cv, cg, taps, gain, ow, res, ids, rw, eg, eu, ed,
    out,
    pk_own, pk_par, tg_own, tg_par, gext, stats, actb, wc, resv, upd, ub, a0s, a1s, gs,
    gath, rows, wgu, wd, acc, ssq, hid, pbuf, sbuf, rbuf, eo, back, xs, xr,
    l_sem, sw_s, sw_r, h_s, h_r, w_s, w_r, st_s, st_r, a_s, a_r, d_s, d_r, g_s, g_r, r_s, r_r,
    b_s, b_r,
):
    sp, tp = lax.axis_index("sp"), lax.axis_index("tp")
    y, c = tp // 2, tp % 2
    other = 1 - c
    partner = (sp, y * 2 + other)
    tok, ch = cv.shape
    half = tok // 2
    width = res.shape[1]
    cols = width // n_y
    ff = eg.shape[2]
    slots = gath.shape[0]
    per = slots // n_sp
    part = slots // 8
    mid = slots // 2

    def column(k):
        return (sp, lax.rem(y + k, n_y) * 2 + c)

    def plane(k):
        return (lax.rem(sp + k, n_sp), tp)

    def remote(src, dst, s, r, dev):
        return pltpu.make_async_remote_copy(
            src_ref=src, dst_ref=dst, send_sem=s, recv_sem=r, device_id=dev, device_id_type=MESH
        )

    my_cols = pl.ds(pl.multiple_of(y * cols, cols), cols)
    my_half = pl.ds(pl.multiple_of(c * half, half), half)
    loads = [
        pltpu.make_async_copy(res.at[my_half, my_cols], resv, l_sem.at[0]),
        pltpu.make_async_copy(eg.at[0], wgu.at[0], l_sem.at[1]),
        pltpu.make_async_copy(eu.at[0], wgu.at[2], l_sem.at[2]),
        pltpu.make_async_copy(ed.at[0], wd.at[pl.ds(0, ff)], l_sem.at[3]),
        pltpu.make_async_copy(
            ow.at[:, my_cols],
            wc.at[y, pl.ds(pl.multiple_of(c * ch, ch), ch)],
            l_sem.at[4],
        ),
    ]
    for load in loads:
        load.start()

    barrier = pltpu.get_barrier_semaphore()

    def greet(dev):
        pl.semaphore_signal(barrier, inc=1, device_id=dev, device_id_type=MESH)

    greet(partner)
    nxt = lax.rem(sp + 1, n_sp)
    prv = lax.rem(sp + n_sp - 1, n_sp)
    greet((nxt, y * 2 + other))
    greet((prv, y * 2 + other))

    @pl.loop(1, n_y)
    def _(k):
        greet(column(k))

    @pl.loop(1, n_sp)
    def _(k):
        greet(plane(k))

    lane = iota((ch, 2 * ch), 1)
    chan = iota((ch, 2 * ch), 0)
    put_low = (lane == chan).astype(BF16)
    put_high = (lane == chan + ch).astype(BF16)
    pk_own[pl.ds(HALO, tok), :] = (matmul(cv[...], put_low) + matmul(cg[...], put_high)).astype(BF16)
    n_taps = taps.shape[0]
    tg_own[...] = jnp.zeros_like(tg_own)
    tg_own[pl.ds(0, n_taps), :] = matmul(taps[...], put_low)
    tg_own[pl.ds(n_taps, 1), :] = matmul(
        jnp.broadcast_to(gain[...], (8, ch)), put_low.astype(F32), lax.Precision.HIGHEST
    )[0:1]

    pl.semaphore_wait(barrier, 3 + (n_y - 1) + (n_sp - 1))

    body = pl.ds(HALO, tok)
    head = pl.ds(0, HALO)
    tail = pl.ds(tok, HALO)
    halo = [
        remote(pk_own.at[tail], pk_own.at[head], h_s.at[0], h_r.at[0], (nxt, tp)),
        remote(pk_own.at[tail], pk_par.at[head], h_s.at[1], h_r.at[1], (nxt, y * 2 + other)),
    ]
    for copy in halo:
        copy.start()
    swap_pk = remote(pk_own.at[body], pk_par.at[body], sw_s.at[0], sw_r.at[0], partner)
    swap_tg = remote(tg_own, tg_par, sw_s.at[1], sw_r.at[1], partner)
    swap_pk.start()
    swap_tg.start()

    def wc_copy(k):
        far = lax.rem(y + k, n_y)
        return remote(
            ow.at[:, pl.ds(pl.multiple_of(far * cols, cols), cols)],
            wc.at[y, pl.ds(pl.multiple_of(c * ch, ch), ch)],
            w_s,
            w_r.at[y],
            column(k),
        )

    @pl.loop(1, n_y)
    def _(k):
        wc_copy(k).start()

    swap_w = [
        remote(eg.at[0], wgu.at[1], sw_s.at[2], sw_r.at[2], partner),
        remote(eu.at[0], wgu.at[3], sw_s.at[3], sw_r.at[3], partner),
        remote(ed.at[0], wd.at[pl.ds(ff, ff)], sw_s.at[4], sw_r.at[4], partner),
    ]
    for copy in swap_w:
        copy.start()

    expert = iota((tok, 128), 1)
    id0, id1 = ids[:, 0:1], ids[:, 1:2]
    hot0, hot1 = (id0 == expert).astype(F32), (id1 == expert).astype(F32)
    before = (iota((tok, tok), 1) < iota((tok, tok), 0)).astype(BF16)
    earlier = matmul(before, (hot0 + hot1).astype(BF16))

    def slot_of(ident, hot):
        rank = jnp.sum(earlier * hot, axis=1, keepdims=True).astype(jnp.int32) - c * per
        return jnp.where((rank >= 0) & (rank < per), ident * per + rank, -1)

    slot0, slot1 = slot_of(id0, hot0), slot_of(id1, hot1)
    place = iota((tok, slots), 1)
    a0s[...] = (place == slot0).astype(BF16)
    a1s[...] = (place == slot1).astype(BF16)

    def along(v):
        return jnp.transpose(jnp.broadcast_to(v.astype(F32), (tok, 128)))[0:1, :]

    row0, row1 = along(slot0), along(slot1)
    place_row = iota((slots, tok), 0).astype(F32)
    gs[...] = jnp.where((place_row == row0) | (place_row == row1), 1.0, 0.0).astype(BF16)

    swap_tg.wait_recv()
    swap_pk.wait_recv()
    for copy in halo:
        copy.wait_recv()
    wide = 2 * ch
    lane2, chan2 = iota((wide, wide), 1), iota((wide, wide), 0)

    def pick(first, to):
        return ((chan2 >= first) & (chan2 < first + ch) & (lane2 == chan2 - first + to * ch)).astype(BF16)

    span = pl.ds(pl.multiple_of(c * half, half), half + HALO)
    mine, theirs = pk_own[span, :], pk_par[span, :]
    value = matmul(mine, pick(0, c)) + matmul(theirs, pick(0, other))
    gate = matmul(mine, pick(ch, c)) + matmul(theirs, pick(ch, other))
    gated = value / (1.0 + jnp.exp(-gate))
    start = (iota(gated.shape, 0) < HALO) & (sp == 0) & (c == 0)
    gext[...] = jnp.where(start, 0.0, gated)
    tg = matmul(tg_own[...], pick(0, c).astype(F32), lax.Precision.HIGHEST) + matmul(
        tg_par[...], pick(0, other).astype(F32), lax.Precision.HIGHEST
    )
    filtered = jnp.zeros((half, wide), F32)
    for i in range(n_taps):
        filtered = filtered + tg[i : i + 1, :] * gext[pl.ds(i + HALO + 1 - n_taps, half), :]

    turned = jnp.transpose(filtered)
    sums = jnp.sum(turned, axis=0, keepdims=True)
    squares = jnp.sum(turned * turned, axis=0, keepdims=True)
    stats[y] = jnp.where(iota((8, half), 0) == 0, sums, squares)

    def st_copy(k):
        return remote(stats.at[y], stats.at[y], st_s, st_r.at[y], column(k))

    @pl.loop(1, n_y)
    def _(k):
        st_copy(k).start()

    @pl.loop(1, n_y)
    def _(k):
        origin = lax.rem(y + k, n_y)
        remote(stats.at[origin], stats.at[origin], st_s, st_r.at[origin], column(k)).wait_recv()

    total = stats[0]
    for o in range(1, n_y):
        total = total + stats[o]
    total = total / (n_y * wide)
    average, power = total[0:1, :], total[1:2, :]
    scale = lax.rsqrt(power - average * average + 1e-05)

    def down(v):
        return jnp.transpose(jnp.broadcast_to(v, (wide, half)))

    normed = (filtered - down(average)) * down(scale) * tg[n_taps : n_taps + 1, :]
    actb[y] = (normed / (1.0 + jnp.exp(-normed))).astype(BF16)

    def a_copy(k):
        return remote(actb.at[y], actb.at[y], a_s, a_r.at[y], column(k))

    @pl.loop(1, n_y)
    def _(k):
        a_copy(k).start()

    own_rows = pl.ds(pl.multiple_of(c * ch, ch), ch)
    loads[4].wait()

    @pl.loop(1, n_y)
    def _(k):
        origin = lax.rem(y + k, n_y)
        remote(
            wc.at[origin, own_rows], wc.at[origin, own_rows], w_s, w_r.at[origin], column(k)
        ).wait_recv()

    swap_wc = remote(wc.at[:, own_rows], wc.at[:, own_rows], sw_s.at[5], sw_r.at[5], partner)
    swap_wc.start()
    loads[0].wait()
    swap_wc.wait_recv()
    upd[...] = resv[...].astype(F32) + matmul(actb[y], wc[y])

    @pl.loop(1, n_y)
    def _(k):
        origin = lax.rem(y + k, n_y)
        remote(actb.at[origin], actb.at[origin], a_s, a_r.at[origin], column(k)).wait_recv()
        upd[...] += matmul(actb[origin], wc[origin])

    ub[my_half, :] = upd[...].astype(BF16)
    swap_ub = remote(ub.at[my_half], ub.at[my_half], sw_s.at[6], sw_r.at[6], partner)
    swap_ub.start()
    swap_ub.wait_recv()

    gath[...] = matmul(gs[...], ub[...]).astype(BF16)

    def at(k):
        return pl.ds(pl.multiple_of(k * per, per), per)

    @pl.loop(1, n_sp)
    def _(k):
        dst = lax.rem(sp + k, n_sp)
        remote(gath.at[at(dst)], rows.at[y, at(sp)], d_s, d_r.at[sp], plane(k)).start()

    keep = pltpu.make_async_copy(gath.at[at(sp)], rows.at[y, at(sp)], d_r.at[sp])
    keep.start()

    for load in loads[1:4]:
        load.wait()
    for copy in swap_w:
        copy.wait_recv()

    def stream(q):
        return pl.ds(q * part, part)

    def turn(q):
        return 1 if q < 4 else -1

    def ring_copy(step, q):
        origin = lax.rem(y + n_y - turn(q) * step, n_y)
        return remote(
            rows.at[origin, stream(q)], rows.at[origin, stream(q)], g_s, g_r.at[step, q],
            column(turn(q) + n_y),
        )

    for q in ORDER:
        for k in range(q * part // per, (q + 1) * part // per):
            pltpu.make_async_copy(rows.at[y, at(k)], rows.at[y, at(k)], d_r.at[k]).wait()
        ring_copy(0, q).start()

    acc[...] = jnp.zeros_like(acc)
    ssq[...] = jnp.zeros_like(ssq)

    def accumulate(origin, first):
        block = pl.ds(first, mid)
        x = rows[origin, block, :]
        xf = x.astype(F32)
        xf = xf * xf
        folded = xf[:, 0:128]
        for j in range(1, cols // 128):
            folded = folded + xf[:, j * 128 : (j + 1) * 128]
        ssq[block, :] += folded
        deep = pl.ds(pl.multiple_of(origin * cols, cols), cols)
        for j in range(4):
            acc[j, block, :] += matmul(x, wgu[j, deep, :])

    accumulate(y, 0)
    accumulate(y, mid)

    @pl.loop(0, n_y - 1)
    def _(step):
        for q in ORDER:
            ring_copy(step, q).wait_recv()

            @pl.when(step < n_y - 2)
            def _():
                ring_copy(step + 1, q).start()

        accumulate(lax.rem(y + n_y - 1 - step, n_y), 0)
        accumulate(lax.rem(y + 1 + step, n_y), mid)

    rms = lax.rsqrt(jnp.sum(ssq[...], axis=1, keepdims=True) / width + 1e-06)
    for j in range(2):
        g = acc[j] * rms
        u = acc[2 + j] * rms
        hid[:, j * ff : (j + 1) * ff] = (g / (1.0 + jnp.exp(-g)) * u).astype(BF16)

    def product(first, chunk):
        block = pl.ds(first, mid)
        at_cols = pl.ds(pl.multiple_of(chunk * cols, cols), cols)
        pbuf[block, :] = matmul(hid[block, :], wd[:, at_cols])

    def sum_copy(step, q):
        return remote(
            sbuf.at[step, stream(q)], rbuf.at[step, stream(q)], r_s, r_r.at[step, q],
            column(turn(q) + n_y),
        )

    product(0, lax.rem(y + n_y - 1, n_y))
    product(mid, lax.rem(y + 1, n_y))
    for q in ORDER:
        sbuf[0, stream(q), :] = pbuf[stream(q), :].astype(BF16)
        sum_copy(0, q).start()

    @pl.loop(1, n_y - 1)
    def _(step):
        product(0, lax.rem(y + n_y - 1 - step, n_y))
        product(mid, lax.rem(y + 1 + step, n_y))
        for q in ORDER:
            sum_copy(step - 1, q).wait_recv()
            both = pbuf[stream(q), :] + rbuf[step - 1, stream(q), :].astype(F32)
            sbuf[step, stream(q), :] = both.astype(BF16)
            sum_copy(step, q).start()

    product(0, y)
    product(mid, y)

    def back_copy(dst):
        return remote(eo.at[at(dst)], back.at[at(sp)], b_s, b_r, (dst, tp))

    for q in ORDER:
        sum_copy(n_y - 2, q).wait_recv()
        both = pbuf[stream(q), :] + rbuf[n_y - 2, stream(q), :].astype(F32)
        eo[stream(q), :] = both.astype(BF16)
        for k in range(q * part // per, (q + 1) * part // per):

            @pl.when(sp != k)
            def _():
                back_copy(jnp.int32(k)).start()

    stay = pltpu.make_async_copy(eo.at[at(sp)], back.at[at(sp)], l_sem.at[5])
    stay.start()
    stay.wait()
    most = pl.ds(0, slots - per)
    pltpu.make_async_copy(back.at[most], back.at[most], b_r).wait()

    w0, w1 = rw[:, 0:1], rw[:, 1:2]
    combined = w0 * matmul(a0s[...], back[...]) + w1 * matmul(a1s[...], back[...])
    xs[0] = combined[:, 0 : cols // 2]
    xs[1] = combined[:, cols // 2 :]
    xs[0, my_half, :] += upd[:, 0 : cols // 2]
    xs[1, my_half, :] += upd[:, cols // 2 :]
    last = remote(xs.at[other], xr, sw_s.at[7], sw_r.at[7], partner)
    last.start()
    last.wait_recv()
    out[...] = (xs[c] + xr[...]).astype(BF16)

    for copy in halo + swap_w + [swap_pk, swap_tg, swap_wc, swap_ub, last]:
        copy.wait_send()
    many = pl.ds(0, n_y - 1)
    pltpu.make_async_copy(wc.at[many, own_rows], wc.at[many, own_rows], w_s).wait()
    pltpu.make_async_copy(stats.at[many], stats.at[many], st_s).wait()
    pltpu.make_async_copy(actb.at[many], actb.at[many], a_s).wait()
    pltpu.make_async_copy(gath.at[most], gath.at[most], d_s).wait()
    pltpu.make_async_copy(rows.at[many], rows.at[many], g_s).wait()
    pltpu.make_async_copy(sbuf, sbuf, r_s).wait()
    pltpu.make_async_copy(eo.at[most], eo.at[most], b_s).wait()


def solution(mesh):
    n_sp, n_y = mesh.shape["sp"], mesh.shape["tp"] // 2

    def local(cv, cg, taps, gain, ow, res, ids, rw, eg, eu, ed):
        tok, ch = cv.shape
        width = res.shape[1]
        cols = width // n_y
        ff = eg.shape[2]
        slots = tok * ids.shape[1]
        half = tok // 2
        vm, hbm = pl.BlockSpec(memory_space=pltpu.VMEM), pl.BlockSpec(memory_space=pl.ANY)
        dma = pltpu.SemaphoreType.DMA
        scratch = [
            pltpu.VMEM((HALO + tok, 2 * ch), BF16),
            pltpu.VMEM((HALO + tok, 2 * ch), BF16),
            pltpu.VMEM((40, 2 * ch), F32),
            pltpu.VMEM((40, 2 * ch), F32),
            pltpu.VMEM((HALO + half, 2 * ch), F32),
            pltpu.VMEM((n_y, 8, half), F32),
            pltpu.VMEM((n_y, half, 2 * ch), BF16),
            pltpu.VMEM((n_y, 2 * ch, cols), BF16),
            pltpu.VMEM((half, cols), BF16),
            pltpu.VMEM((half, cols), F32),
            pltpu.VMEM((tok, cols), BF16),
            pltpu.VMEM((tok, slots), BF16),
            pltpu.VMEM((tok, slots), BF16),
            pltpu.VMEM((slots, tok), BF16),
            pltpu.VMEM((slots, cols), BF16),
            pltpu.VMEM((n_y, slots, cols), BF16),
            pltpu.VMEM((4, width, ff), BF16),
            pltpu.VMEM((2 * ff, width), BF16),
            pltpu.VMEM((4, slots, ff), F32),
            pltpu.VMEM((slots, 128), F32),
            pltpu.VMEM((slots, 2 * ff), BF16),
            pltpu.VMEM((slots, cols), F32),
            pltpu.VMEM((n_y - 1, slots, cols), BF16),
            pltpu.VMEM((n_y - 1, slots, cols), BF16),
            pltpu.VMEM((slots, cols), BF16),
            pltpu.VMEM((slots, cols), BF16),
            pltpu.VMEM((2, tok, cols // 2), F32),
            pltpu.VMEM((tok, cols // 2), F32),
            dma((6,)), dma((8,)), dma((8,)), dma((2,)), dma((2,)),
            dma, dma((n_y,)), dma, dma((n_y,)), dma, dma((n_y,)),
            dma, dma((n_sp,)), dma, dma((n_y - 1, 8)), dma, dma((n_y - 1, 8)),
            dma, dma,
        ]
        return pl.pallas_call(
            functools.partial(layer, n_sp, n_y),
            out_shape=jax.ShapeDtypeStruct((tok, cols // 2), BF16),
            in_specs=[vm, vm, vm, vm, hbm, hbm, vm, vm, hbm, hbm, hbm],
            out_specs=vm,
            scratch_shapes=scratch,
            compiler_params=pltpu.CompilerParams(
                collective_id=0, has_side_effects=True, vmem_limit_bytes=56 << 20
            ),
        )(cv, cg, taps, gain.reshape(1, ch), ow, res, ids, rw, eg, eu, ed)

    placed = (
        P("sp", "tp"), P("sp", "tp"), P(None, "tp"), P("tp"), P("tp", None), P("sp", None),
        P("sp", None), P("sp", None), P("sp", None, "tp"), P("sp", None, "tp"), P("sp", "tp", None),
    )
    return jax.shard_map(local, mesh=mesh, in_specs=placed, out_specs=P("sp", "tp"), check_vma=False)
```

time: 287 us -> 113 us (0.39)
  blocking collectives: 112 us -> 0 us
  Pallas kernels: 0 us -> 108 us
  waiting for transfers between devices: 79.9 us -> 0 us
  local copies, waits for them, and re-layouts: 36.6 us -> 5.3 us
  starting transfers between devices: 24 us -> 0 us
  between operations: 13.8 us -> 0.01 us
  other arithmetic: 13.7 us -> 0 us
  matrix products: 4.37 us -> 0 us
    all_to_all x6 -> x0, blocking collectives: 112 us -> none  [the longest x1 54.1 us: sum_in_two_steps(): lax.all_to_all(nearer.astype(jnp.bfloat16), far, split_axis=0, concat_axi...]
    pallas_call x0 -> x1, Pallas kernels: none -> 108 us  [local(): pl.pallas_call(functools.partial(layer, n_sp, n_y), out_shape=jax.ShapeDt...]
    all_to_all x3 -> x0, waiting for transfers between devices: 43.3 us -> none  [the longest x1 17.5 us: sent_to_all(): lax.all_to_all(jnp.broadcast_to(value[None], (size, *value.shape)), axis,...]
    all_gather x1 -> x0, waiting for transfers between devices: 36.6 us -> none  [local(): block = lax.all_gather(arrived, TP, axis=1, tiled=True)]
    all_to_all x3 -> x0, starting transfers between devices: 16.9 us -> none  [the longest x1 9.9 us: local(): back = lax.all_to_all(summed, 'sp', split_axis=0, concat_axis=0, tiled=True)]
    reshape x3 -> x0, local copies, waits for them, and re-layouts: 9.58 us -> none  [the longest x2 9.44 us: split_up(): value.reshape(*shape[:dim], size, shape[dim] // size, *shape[dim + 1:])]
    reduce_sum x10 -> x0, other arithmetic: 7.61 us -> none  [the longest x2 4.42 us: summed_on_arrival(): return jnp.sum(blocks.astype(jnp.float32), axis=0)]
    gather x2 -> x0, local copies, waits for them, and re-layouts: 7.35 us -> none  [the longest x1 6.02 us: local(): buffer = padded_rows[holders].reshape(experts, capacity, width)]
  transfers between devices with their start and end apart: 6 -> 0, of which waited for: 4 -> 0; matrix products, arithmetic and copies ran while one was open for 2% -> 0% of each run, Pallas kernels for 0% -> 0%
where the time goes in v1:
time: 113 us
  Pallas kernels  108 us (96%)
  local copies, waits for them, and re-layouts  5.3 us (5%)
    pallas_call x1, Pallas kernels, local(): pl.pallas_call(functools.partial(layer, n_sp, n_y), out_shape=jax.ShapeDt...  108 us
    unnamed x11, local copies, waits for them, and re-layouts  5.3 us

profile of v1, /device:TPU:1, one launch (start us, length us, event | category | flops | bytes accessed | tf_op | source)
XLA Modules:
  0.0 113.1 jit_solution(9359871566490091757)
XLA Ops:
  0.0 0.0 copy-start
  0.0 1.5 %copy.12.cv = bf16[256,64]{1,0:T(8,128)(2,1)} copy(bf16[256,64]{0,1:T(8,128)(2,1)} %param.11) | data formatting | bytes 65536 | tf_op args[0]
  1.5 0.0 copy-done
  1.5 0.0 copy-start.1
  1.5 0.7 copy.13.cg
  2.2 0.0 copy-done.1
  2.2 0.0 copy-start.2
  2.2 0.8 copy.14.ids
  3.0 0.0 copy-done.2
  3.0 0.8 copy.15.rw
  3.8 107.8 %shard_map.109 = bf16[256,128]{1,0:T(8,128)(2,1)} custom-call(bf16[256,64]{1,0:T(8,128)(2,1)} %copy.12.cv, bf16[256,64]{1,0:T(8,128)(2,1)} %copy.13.cg, bf16[31,64]{1,0:T(8,128)(2,1)} %taps.1, f32[1,64]{1,0:T(1,128)} %bitcast.1, bf16[64,2048]{1,0:T(8,128)(2,1)} %ow.1, bf16[256,2048]{1,0:T(8,128)(2,1)} %res.1, s32[256,2]{1,0:T(8,128)} %copy.14.ids, ...), custom_call_target="tpu_custom_call" | custom-call | tf_op jit(solution)/shard_map/pallas_call | solution.py:444
  111.6 1.5 %copy.17 = bf16[256,128]{1,0:T(8,128)(2,1)} copy(bf16[256,128]{1,0:T(8,128)(2,1)} %shard_map.109) | data formatting | bytes 131072
Async XLA Ops:
  0.0 1.5 %copy-start = (bf16[256,64]{0,1:T(8,128)(2,1)S(1)}, bf16[256,64]{0,1:T(8,128)(2,1)}, u32[]{:S(2)}) copy-start(bf16[256,64]{0,1:T(8,128)(2,1)} %param.12) | copy-start | bytes 98308
  1.5 0.7 copy-start.1
  2.2 0.8 copy-start.2

commit v2 on v1

v2 whole, which is shorter than its diff:
```python
import functools

import jax
import jax.numpy as jnp
from jax import lax
from jax.experimental import pallas as pl
from jax.experimental.pallas import tpu as pltpu
from jax.sharding import PartitionSpec as P

MESH = pl.DeviceIdType.MESH
F32, BF16 = jnp.float32, jnp.bfloat16
HALO = 32
STREAMS = 8
PAIRS = ((0, 7), (1, 6), (2, 5), (3, 4))
ORDER = (0, 7, 1, 6, 2, 5, 3, 4)


def iota(shape, dim):
    return lax.broadcasted_iota(jnp.int32, shape, dim)


def matmul(a, b, precision=None):
    return jnp.dot(a, b, preferred_element_type=F32, precision=precision)


def matmul_t(a, b):
    return lax.dot_general(a, b, (((0,), (0,)), ((), ())), preferred_element_type=F32)


def layer(
    n_sp, n_y,
    cv, cg, taps, gain, ow, res, ids, rw, eg, eu, ed,
    out,
    pk_own, pk_par, tg_own, tg_par, gext, stats, gains, gcol, devs, wc, resv, upd, ub, gs, wts,
    gath, rows, wgu, wd, acc, ssq, hid, sbuf, rbuf, eo, back, xs, xr,
    l_sem, sw_s, sw_r, h_s, h_r, w_s, w_r, st_s, st_r, a_s, a_r, gn_s, gn_r, d_s, d_r, g_s, g_r,
    r_s, r_r, b_s, b_r,
):
    sp, tp = lax.axis_index("sp"), lax.axis_index("tp")
    y, c = tp // 2, tp % 2
    other = 1 - c
    n_x = n_sp // STREAMS
    z, x = sp // n_x, sp % n_x
    partner = (sp, y * 2 + other)
    ch, tok = cv.shape
    half = tok // 2
    wide = 2 * ch
    width = res.shape[1]
    cols = width // n_y
    ff = eg.shape[2]
    slots = gath.shape[0]
    per = slots // n_sp
    part = slots // STREAMS
    mid = slots // 2

    def column(k):
        return (sp, lax.rem(y + k, n_y) * 2 + c)

    def remote(src, dst, s, r, dev):
        return pltpu.make_async_remote_copy(
            src_ref=src, dst_ref=dst, send_sem=s, recv_sem=r, device_id=dev, device_id_type=MESH
        )

    my_cols = pl.ds(pl.multiple_of(y * cols, cols), cols)
    my_half = pl.ds(pl.multiple_of(c * half, half), half)
    own_rows = pl.ds(pl.multiple_of(c * ch, ch), ch)
    loads = [
        pltpu.make_async_copy(res.at[my_half, my_cols], resv, l_sem.at[0]),
        pltpu.make_async_copy(eg.at[0], wgu.at[0], l_sem.at[1]),
        pltpu.make_async_copy(eu.at[0], wgu.at[2], l_sem.at[2]),
        pltpu.make_async_copy(ed.at[0], wd.at[pl.ds(0, ff)], l_sem.at[3]),
        pltpu.make_async_copy(ow.at[:, my_cols], wc.at[y, own_rows], l_sem.at[4]),
    ]
    for load in loads:
        load.start()

    barrier = pltpu.get_barrier_semaphore()

    def greet(dev):
        pl.semaphore_signal(barrier, inc=1, device_id=dev, device_id_type=MESH)

    nxt = lax.rem(sp + 1, n_sp)
    prv = lax.rem(sp + n_sp - 1, n_sp)

    @pl.loop(1, n_sp)
    def _(k):
        greet((lax.rem(sp + k, n_sp), tp))

    @pl.loop(1, n_y)
    def _(k):
        greet(column(k))

    greet((nxt, y * 2 + other))
    greet((prv, y * 2 + other))
    greet(partner)

    lane = iota((ch, wide), 1)
    chan = iota((ch, wide), 0)
    put_low = (lane == chan).astype(BF16)
    put_high = (lane == chan + ch).astype(BF16)
    pk_own[pl.ds(HALO, tok), :] = (
        matmul_t(cv[...], put_low) + matmul_t(cg[...], put_high)
    ).astype(BF16)
    n_taps = taps.shape[0]
    tg_own[...] = jnp.zeros_like(tg_own)
    tg_own[pl.ds(0, n_taps), :] = matmul(taps[...], put_low)
    tg_own[pl.ds(n_taps, 1), :] = matmul(
        jnp.broadcast_to(gain[...], (8, ch)), put_low.astype(F32), lax.Precision.HIGHEST
    )[0:1]

    expert = iota((128, tok), 0)
    id0, id1 = ids[0:1, :], ids[1:2, :]
    hot0, hot1 = (id0 == expert).astype(F32), (id1 == expert).astype(F32)
    before = (iota((tok, tok), 0) < iota((tok, tok), 1)).astype(BF16)
    earlier = matmul((hot0 + hot1).astype(BF16), before)
    place = iota((slots, tok), 0)
    for k, (ident, hot) in enumerate(((id0, hot0), (id1, hot1))):
        rank = jnp.sum(earlier * hot, axis=0, keepdims=True).astype(jnp.int32) - c * per
        slot = jnp.where((rank >= 0) & (rank < per), ident * per + rank, -1)
        gs[k] = jnp.where(place == slot, 1.0, 0.0).astype(BF16)
        wts[k] = jnp.transpose(jnp.broadcast_to(rw[k : k + 1, :], (128, tok)))

    pl.semaphore_wait(barrier, 3 + (n_y - 1) + (n_sp - 1))

    body = pl.ds(HALO, tok)
    head = pl.ds(0, HALO)
    tail = pl.ds(tok, HALO)
    halo = [
        remote(pk_own.at[tail], pk_own.at[head], h_s.at[0], h_r.at[0], (nxt, tp)),
        remote(pk_own.at[tail], pk_par.at[head], h_s.at[1], h_r.at[1], (nxt, y * 2 + other)),
    ]
    for copy in halo:
        copy.start()
    swap_tg = remote(tg_own, tg_par, sw_s.at[1], sw_r.at[1], partner)
    swap_pk = remote(pk_own.at[body], pk_par.at[body], sw_s.at[0], sw_r.at[0], partner)
    swap_tg.start()
    swap_pk.start()

    @pl.loop(1, n_y)
    def _(k):
        far = lax.rem(y + k, n_y)
        far_cols = pl.ds(pl.multiple_of(far * cols, cols), cols)
        remote(ow.at[:, far_cols], wc.at[y, own_rows], w_s, w_r.at[y], column(k)).start()

    swap_w = [
        remote(eg.at[0], wgu.at[1], sw_s.at[2], sw_r.at[2], partner),
        remote(eu.at[0], wgu.at[3], sw_s.at[3], sw_r.at[3], partner),
        remote(ed.at[0], wd.at[pl.ds(ff, ff)], sw_s.at[4], sw_r.at[4], partner),
    ]
    for copy in swap_w:
        copy.start()

    lane2, chan2 = iota((wide, wide), 1), iota((wide, wide), 0)

    def pick(first, to):
        return (
            (chan2 >= first) & (chan2 < first + ch) & (lane2 == chan2 - first + to * ch)
        ).astype(BF16)

    swap_tg.wait_recv()
    tg = matmul(tg_own[...], pick(0, c).astype(F32), lax.Precision.HIGHEST) + matmul(
        tg_par[...], pick(0, other).astype(F32), lax.Precision.HIGHEST
    )

    def everywhere(buf, s, r):
        @pl.loop(1, n_y)
        def _(k):
            remote(buf.at[y], buf.at[y], s, r.at[y], column(k)).start()

    def arrived(buf, s, r, k):
        origin = lax.rem(y + k, n_y)
        remote(buf.at[origin], buf.at[origin], s, r.at[origin], column(k)).wait_recv()
        return origin

    swap_pk.wait_recv()
    for copy in halo:
        copy.wait_recv()
    span = pl.ds(pl.multiple_of(c * half, half), half + HALO)
    mine, theirs = pk_own[span, :], pk_par[span, :]
    value = matmul(mine, pick(0, c)) + matmul(theirs, pick(0, other))
    gate = matmul(mine, pick(ch, c)) + matmul(theirs, pick(ch, other))
    gated = value / (1.0 + jnp.exp(-gate))
    start = (iota(gated.shape, 0) < HALO) & (sp == 0) & (c == 0)
    gext[...] = jnp.where(start, 0.0, gated)
    filtered = jnp.zeros((half, wide), F32)
    for i in range(n_taps):
        filtered = filtered + tg[i : i + 1, :] * gext[pl.ds(i + HALO + 1 - n_taps, half), :]

    turned = jnp.transpose(filtered)
    mean = jnp.sum(turned, axis=0, keepdims=True) / wide
    turned = turned - mean
    spread = jnp.sum(turned * turned, axis=0, keepdims=True) / wide
    devs[y] = turned.astype(BF16)
    stats[y] = jnp.where(iota((8, half), 0) == 0, mean, spread)
    gains[y] = jnp.broadcast_to(tg[n_taps : n_taps + 1, :], (8, wide))
    everywhere(stats, st_s, st_r)
    everywhere(gains, gn_s, gn_r)
    everywhere(devs, a_s, a_r)

    loads[4].wait()

    @pl.loop(1, n_y)
    def _(k):
        origin = lax.rem(y + k, n_y)
        remote(
            wc.at[origin, own_rows], wc.at[origin, own_rows], w_s, w_r.at[origin], column(k)
        ).wait_recv()

    swap_wc = remote(wc.at[:, own_rows], wc.at[:, own_rows], sw_s.at[5], sw_r.at[5], partner)
    swap_wc.start()

    @pl.loop(1, n_y)
    def _(k):
        arrived(stats, st_s, st_r, k)
        arrived(gains, gn_s, gn_r, k)

    average = stats[0, 0:1, :]
    for o in range(1, n_y):
        average = average + stats[o, 0:1, :]
    average = average / n_y
    variance = jnp.zeros_like(average)
    for o in range(n_y):
        gap = stats[o, 0:1, :] - average
        variance = variance + (stats[o, 1:2, :] + gap * gap)
    scale = lax.rsqrt(variance / n_y + 1e-05)
    for o in range(n_y):
        gcol[o] = jnp.transpose(jnp.broadcast_to(gains[o, 0:1, :], (half, wide))) * scale

    def mixed(origin):
        shift = stats[origin, 0:1, :] - average
        normed = (devs[origin].astype(F32) + shift) * gcol[origin]
        activated = (normed / (1.0 + jnp.exp(-normed))).astype(BF16)
        return matmul_t(activated, wc[origin])

    loads[0].wait()
    swap_wc.wait_recv()
    upd[...] = resv[...].astype(F32) + mixed(y)
    for k in (1, 7, 2, 6, 3, 5, 4) if n_y == 8 else range(1, n_y):
        upd[...] += mixed(arrived(devs, a_s, a_r, k))

    ub[my_half, :] = upd[...].astype(BF16)
    swap_ub = remote(ub.at[my_half], ub.at[my_half], sw_s.at[6], sw_r.at[6], partner)
    swap_ub.start()
    swap_ub.wait_recv()

    gath[...] = matmul(gs[0] + gs[1], ub[...]).astype(BF16)

    def at(k):
        return pl.ds(pl.multiple_of(k * per, per), per)

    def below(j):
        return lax.rem(z + STREAMS - j, STREAMS)

    def above(j):
        return lax.rem(z + j, STREAMS)

    for j in ORDER:
        spot = j * n_x + x
        for i in range(n_x):
            dst = below(j) * n_x + lax.rem(x + i, n_x)
            if i == 0 and j == 0:
                keep = pltpu.make_async_copy(gath.at[at(dst)], rows.at[y, at(spot)], d_r.at[spot])
                keep.start()
            else:
                remote(gath.at[at(dst)], rows.at[y, at(spot)], d_s, d_r.at[spot], (dst, tp)).start()

    for load in loads[1:4]:
        load.wait()
    for copy in swap_w:
        copy.wait_recv()
    acc[...] = jnp.zeros_like(acc)
    ssq[...] = jnp.zeros_like(ssq)

    def stream(j):
        return pl.ds(j * part, part)

    def turn(j):
        return 1 if j < STREAMS // 2 else -1

    def source(step, j):
        return lax.rem(y + n_y - turn(j) * step, n_y)

    def ring_copy(step, j):
        origin = source(step, j)
        return remote(
            rows.at[origin, stream(j)], rows.at[origin, stream(j)], g_s, g_r.at[step, j],
            column(turn(j) + n_y),
        )

    def deep(origin):
        return pl.ds(pl.multiple_of(origin * cols, cols), cols)

    def folded(v):
        v = v.astype(F32)
        v = v * v
        total = v[:, 0:128]
        for i in range(1, cols // 128):
            total = total + v[:, i * 128 : (i + 1) * 128]
        return total

    def accumulate(origin, block):
        v = rows[origin, block, :]
        ssq[block, :] += folded(v)
        for i in range(4):
            acc[i, block, :] += matmul(v, wgu[i, deep(origin), :])

    early = 4

    def finish(j):
        block = stream(j)
        for step in range(early + 1, n_y):
            accumulate(source(step, j), block)
        rms = lax.rsqrt(jnp.sum(ssq[block, :], axis=1, keepdims=True) / width + 1e-06)
        for i in range(2):
            g = acc[i, block, :] * rms
            u = acc[2 + i, block, :] * rms
            hid[block, i * ff : (i + 1) * ff] = (g / (1.0 + jnp.exp(-g)) * u).astype(BF16)

    def sum_copy(step, j):
        return remote(
            sbuf.at[step, stream(j)], rbuf.at[step, stream(j)], r_s, r_r.at[step, j],
            column(turn(j) + n_y),
        )

    def product(step, j):
        chunk = source(step + 1, j)
        return matmul(hid[stream(j), :], wd[:, pl.ds(pl.multiple_of(chunk * cols, cols), cols)])

    def send_sum(step, j):
        partial = product(step, j)
        if step > 0:
            sum_copy(step - 1, j).wait_recv()
            partial = partial + rbuf[step - 1, stream(j), :].astype(F32)
        sbuf[step, stream(j), :] = partial.astype(BF16)
        sum_copy(step, j).start()

    def send_back(j):
        partial = product(n_y - 1, j)
        sum_copy(n_y - 2, j).wait_recv()
        eo[stream(j), :] = (partial + rbuf[n_y - 2, stream(j), :].astype(F32)).astype(BF16)
        for i in range(n_x):
            spot = j * n_x + i
            dst = above(j) * n_x + i
            if j == 0:

                @pl.when(x != i)
                def _():
                    remote(eo.at[at(spot)], back.at[at(sp)], b_s, b_r, (dst, tp)).start()

            else:
                remote(eo.at[at(spot)], back.at[at(sp)], b_s, b_r, (dst, tp)).start()

    lag = len(PAIRS) - 1
    for t in range(-1, 2 * n_y + lag + 1):
        for i, pair in enumerate(PAIRS):
            step = t - i
            for j in pair:
                if step == -1:
                    for k in range(j * n_x, (j + 1) * n_x):
                        spot = rows.at[y, at(k)]
                        pltpu.make_async_copy(spot, spot, d_r.at[k]).wait()
                    ring_copy(0, j).start()
                elif 0 <= step < n_y - 1:
                    ring_copy(step, j).wait_recv()
                    if step < n_y - 2:
                        ring_copy(step + 1, j).start()
        done = t - lag + 1
        if 0 <= done <= early:
            accumulate(source(done, 0), pl.ds(0, mid))
            accumulate(source(done, STREAMS - 1), pl.ds(mid, mid))
        for i, pair in enumerate(PAIRS):
            step = t - i - (n_y - 2)
            for j in pair:
                if step == 0:
                    finish(j)
                if 0 <= step < n_y - 1:
                    send_sum(step, j)
                elif step == n_y - 1:
                    send_back(j)

    stay = pltpu.make_async_copy(eo.at[at(x)], back.at[at(sp)], l_sem.at[5])
    stay.start()
    stay.wait()
    most = pl.ds(0, slots - per)
    pltpu.make_async_copy(back.at[most], back.at[most], b_r).wait()

    first, second = matmul_t(gs[0], back[...]), matmul_t(gs[1], back[...])
    for i in range(2):
        lanes = slice(i * (cols // 2), (i + 1) * (cols // 2))
        xs[i] = wts[0] * first[:, lanes] + wts[1] * second[:, lanes]
        xs[i, my_half, :] += upd[:, lanes]
    last = remote(xs.at[other], xr, sw_s.at[7], sw_r.at[7], partner)
    last.start()
    last.wait_recv()
    out[...] = (xs[c] + xr[...]).astype(BF16)

    for copy in halo + swap_w + [swap_pk, swap_tg, swap_wc, swap_ub, last]:
        copy.wait_send()
    many = pl.ds(0, n_y - 1)
    pltpu.make_async_copy(wc.at[many, own_rows], wc.at[many, own_rows], w_s).wait()
    pltpu.make_async_copy(stats.at[many], stats.at[many], st_s).wait()
    pltpu.make_async_copy(gains.at[many], gains.at[many], gn_s).wait()
    pltpu.make_async_copy(devs.at[many], devs.at[many], a_s).wait()
    pltpu.make_async_copy(gath.at[most], gath.at[most], d_s).wait()
    pltpu.make_async_copy(rows.at[many], rows.at[many], g_s).wait()
    pltpu.make_async_copy(sbuf, sbuf, r_s).wait()
    pltpu.make_async_copy(eo.at[most], eo.at[most], b_s).wait()


def solution(mesh):
    n_sp, n_y = mesh.shape["sp"], mesh.shape["tp"] // 2

    def local(cv, cg, taps, gain, ow, res, ids, rw, eg, eu, ed):
        tok, ch = cv.shape
        width = res.shape[1]
        cols = width // n_y
        ff = eg.shape[2]
        slots = tok * ids.shape[1]
        half = tok // 2
        vm, hbm = pl.BlockSpec(memory_space=pltpu.VMEM), pl.BlockSpec(memory_space=pl.ANY)
        dma = pltpu.SemaphoreType.DMA
        scratch = [
            pltpu.VMEM((HALO + tok, 2 * ch), BF16),
            pltpu.VMEM((HALO + tok, 2 * ch), BF16),
            pltpu.VMEM((40, 2 * ch), F32),
            pltpu.VMEM((40, 2 * ch), F32),
            pltpu.VMEM((HALO + half, 2 * ch), F32),
            pltpu.VMEM((n_y, 8, half), F32),
            pltpu.VMEM((n_y, 8, 2 * ch), F32),
            pltpu.VMEM((n_y, 2 * ch, half), F32),
            pltpu.VMEM((n_y, 2 * ch, half), BF16),
            pltpu.VMEM((n_y, 2 * ch, cols), BF16),
            pltpu.VMEM((half, cols), BF16),
            pltpu.VMEM((half, cols), F32),
            pltpu.VMEM((tok, cols), BF16),
            pltpu.VMEM((2, slots, tok), BF16),
            pltpu.VMEM((2, tok, 128), F32),
            pltpu.VMEM((slots, cols), BF16),
            pltpu.VMEM((n_y, slots, cols), BF16),
            pltpu.VMEM((4, width, ff), BF16),
            pltpu.VMEM((2 * ff, width), BF16),
            pltpu.VMEM((4, slots, ff), F32),
            pltpu.VMEM((slots, 128), F32),
            pltpu.VMEM((slots, 2 * ff), BF16),
            pltpu.VMEM((n_y - 1, slots, cols), BF16),
            pltpu.VMEM((n_y - 1, slots, cols), BF16),
            pltpu.VMEM((slots, cols), BF16),
            pltpu.VMEM((slots, cols), BF16),
            pltpu.VMEM((2, tok, cols // 2), F32),
            pltpu.VMEM((tok, cols // 2), F32),
            dma((6,)), dma((8,)), dma((8,)), dma((2,)), dma((2,)),
            dma, dma((n_y,)), dma, dma((n_y,)), dma, dma((n_y,)), dma, dma((n_y,)),
            dma, dma((n_sp,)), dma, dma((n_y - 1, 8)), dma, dma((n_y - 1, 8)),
            dma, dma,
        ]
        return pl.pallas_call(
            functools.partial(layer, n_sp, n_y),
            out_shape=jax.ShapeDtypeStruct((tok, cols // 2), BF16),
            in_specs=[vm, vm, vm, vm, hbm, hbm, vm, vm, hbm, hbm, hbm],
            out_specs=vm,
            scratch_shapes=scratch,
            compiler_params=pltpu.CompilerParams(
                collective_id=0, has_side_effects=True, vmem_limit_bytes=56 << 20
            ),
        )(cv.T, cg.T, taps, gain.reshape(1, ch), ow, res, ids.T, rw.T, eg, eu, ed)

    placed = (
        P("sp", "tp"), P("sp", "tp"), P(None, "tp"), P("tp"), P("tp", None), P("sp", None),
        P("sp", None), P("sp", None), P("sp", None, "tp"), P("sp", None, "tp"), P("sp", "tp", None),
    )
    return jax.shard_map(local, mesh=mesh, in_specs=placed, out_specs=P("sp", "tp"), check_vma=False)
```

time: 113 us -> 119 us (1.053)
  Pallas kernels: 108 us -> 117 us
  local copies, waits for them, and re-layouts: 5.3 us -> 1.47 us
    pallas_call x1, Pallas kernels: 108 us -> 117 us  [local(): pl.pallas_call(functools.partial(layer, n_sp, n_y), out_shape=jax.ShapeDt...]
    unnamed x11 -> x1, local copies, waits for them, and re-layouts: 5.3 us -> 1.47 us
where the time goes in v2:
time: 119 us
  Pallas kernels  117 us (98%)
  local copies, waits for them, and re-layouts  1.47 us (1%)
    pallas_call x1, Pallas kernels, local(): pl.pallas_call(functools.partial(layer, n_sp, n_y), out_shape=jax.ShapeDt...  117 us

profile of v2, /device:TPU:1, one launch (start us, length us, event | category | flops | bytes accessed | tf_op | source)
XLA Modules:
  0.0 118.8 jit_solution(6275830515785078585)
XLA Ops:
  0.0 117.3 %shard_map.109 = bf16[256,128]{1,0:T(8,128)(2,1)} custom-call(bf16[64,256]{1,0:T(8,128)(2,1)} %bitcast.5, bf16[64,256]{1,0:T(8,128)(2,1)} %bitcast.6, bf16[31,64]{1,0:T(8,128)(2,1)} %taps.1, f32[1,64]{1,0:T(1,128)} %bitcast.9, bf16[64,2048]{1,0:T(8,128)(2,1)} %ow.1, bf16[256,2048]{1,0:T(8,128)(2,1)} %res.1, s32[2,256]{1,0:T(2,128)} %bitcast.7, ...), custom_call_target="tpu_custom_call" | custom-call | tf_op jit(solution)/shard_map/pallas_call | solution.py:456
  117.3 1.5 %copy.13 = bf16[256,128]{1,0:T(8,128)(2,1)} copy(bf16[256,128]{1,0:T(8,128)(2,1)} %shard_map.109) | data formatting | bytes 131072

commit v3 on v2

--- a/solution.py
+++ b/solution.py
@@ -11,7 +11,7 @@
 F32, BF16 = jnp.float32, jnp.bfloat16
 HALO = 32
 STREAMS = 8
-PAIRS = ((0, 7), (1, 6), (2, 5), (3, 4))
+UNITS = 4
 ORDER = (0, 7, 1, 6, 2, 5, 3, 4)
 
 
@@ -50,8 +50,8 @@
     ff = eg.shape[2]
     slots = gath.shape[0]
     per = slots // n_sp
-    part = slots // STREAMS
-    mid = slots // 2
+    size = slots // UNITS
+    far = n_y // 2
 
     def column(k):
         return (sp, lax.rem(y + k, n_y) * 2 + c)
@@ -138,8 +138,8 @@
 
     @pl.loop(1, n_y)
     def _(k):
-        far = lax.rem(y + k, n_y)
-        far_cols = pl.ds(pl.multiple_of(far * cols, cols), cols)
+        dst_chip = lax.rem(y + k, n_y)
+        far_cols = pl.ds(pl.multiple_of(dst_chip * cols, cols), cols)
         remote(ow.at[:, far_cols], wc.at[y, own_rows], w_s, w_r.at[y], column(k)).start()
 
     swap_w = [
@@ -254,8 +254,8 @@
     def above(j):
         return lax.rem(z + j, STREAMS)
 
-    for j in ORDER:
-        spot = j * n_x + x
+    for place_j, j in enumerate(ORDER):
+        spot = place_j * n_x + x
         for i in range(n_x):
             dst = below(j) * n_x + lax.rem(x + i, n_x)
             if i == 0 and j == 0:
@@ -271,21 +271,24 @@
     acc[...] = jnp.zeros_like(acc)
     ssq[...] = jnp.zeros_like(ssq)
 
-    def stream(j):
-        return pl.ds(j * part, part)
-
-    def turn(j):
-        return 1 if j < STREAMS // 2 else -1
-
-    def source(step, j):
-        return lax.rem(y + n_y - turn(j) * step, n_y)
-
-    def ring_copy(step, j):
-        origin = source(step, j)
-        return remote(
-            rows.at[origin, stream(j)], rows.at[origin, stream(j)], g_s, g_r.at[step, j],
-            column(turn(j) + n_y),
-        )
+    def unit(u):
+        return pl.ds(u * size, size)
+
+    def piece(u, d):
+        return pl.ds(u * size + d * (size // 2), size // 2)
+
+    def chip(k):
+        return lax.rem(y + n_y + k, n_y)
+
+    def hop(h, d, u):
+        origin = chip(1 - h if d == 0 else h - 1)
+        block = rows.at[origin, unit(u) if h < far else piece(u, d)]
+        return remote(block, block, g_s, g_r.at[d, h - 1, u], column(1 if d == 0 else n_y - 1))
+
+    def hop_in(h, d, u):
+        origin = chip(-h if d == 0 else h)
+        block = rows.at[origin, unit(u) if h < far else piece(u, d)]
+        return remote(block, block, g_s, g_r.at[d, h - 1, u], partner)
 
     def deep(origin):
         return pl.ds(pl.multiple_of(origin * cols, cols), cols)
@@ -304,79 +307,102 @@
         for i in range(4):
             acc[i, block, :] += matmul(v, wgu[i, deep(origin), :])
 
-    early = 4
-
-    def finish(j):
-        block = stream(j)
-        for step in range(early + 1, n_y):
-            accumulate(source(step, j), block)
+    def finish(u):
+        block = unit(u)
+        for origin in (chip(1 - far), chip(far - 1), chip(far)):
+            accumulate(origin, block)
         rms = lax.rsqrt(jnp.sum(ssq[block, :], axis=1, keepdims=True) / width + 1e-06)
         for i in range(2):
             g = acc[i, block, :] * rms
-            u = acc[2 + i, block, :] * rms
-            hid[block, i * ff : (i + 1) * ff] = (g / (1.0 + jnp.exp(-g)) * u).astype(BF16)
-
-    def sum_copy(step, j):
+            v = acc[2 + i, block, :] * rms
+            hid[block, i * ff : (i + 1) * ff] = (g / (1.0 + jnp.exp(-g)) * v).astype(BF16)
+
+    def product(u, chunk):
+        return matmul(hid[unit(u), :], wd[:, deep(chunk)])
+
+    def sum_copy(r, d, u):
+        block = unit(u) if r > 0 else piece(u, d)
         return remote(
-            sbuf.at[step, stream(j)], rbuf.at[step, stream(j)], r_s, r_r.at[step, j],
-            column(turn(j) + n_y),
+            sbuf.at[d, r, block], rbuf.at[d, r, block], r_s, r_r.at[d, r, u],
+            column(1 if d == 0 else n_y - 1),
         )
 
-    def product(step, j):
-        chunk = source(step + 1, j)
-        return matmul(hid[stream(j), :], wd[:, pl.ds(pl.multiple_of(chunk * cols, cols), cols)])
-
-    def send_sum(step, j):
-        partial = product(step, j)
-        if step > 0:
-            sum_copy(step - 1, j).wait_recv()
-            partial = partial + rbuf[step - 1, stream(j), :].astype(F32)
-        sbuf[step, stream(j), :] = partial.astype(BF16)
-        sum_copy(step, j).start()
-
-    def send_back(j):
-        partial = product(n_y - 1, j)
-        sum_copy(n_y - 2, j).wait_recv()
-        eo[stream(j), :] = (partial + rbuf[n_y - 2, stream(j), :].astype(F32)).astype(BF16)
-        for i in range(n_x):
-            spot = j * n_x + i
-            dst = above(j) * n_x + i
-            if j == 0:
-
-                @pl.when(x != i)
-                def _():
+    def first_sums(u):
+        partial = product(u, chip(far)).astype(BF16)
+        for d in range(2):
+            sbuf[d, 0, piece(u, d), :] = partial[d * (size // 2) : (d + 1) * (size // 2)]
+            sum_copy(0, d, u).start()
+
+    def next_sums(r, u):
+        for d in range(2):
+            partial = product(u, chip(far - r if d == 0 else r - far))
+            sum_copy(r - 1, d, u).wait_recv()
+            if r == 1:
+                here, there = (piece(u, 0), piece(u, 1)) if d == 0 else (piece(u, 1), piece(u, 0))
+                parts = (partial[0 : size // 2], partial[size // 2 :])
+                sbuf[d, r, here, :] = (parts[d] + rbuf[d, 0, here, :].astype(F32)).astype(BF16)
+                sbuf[d, r, there, :] = parts[1 - d].astype(BF16)
+            else:
+                partial = partial + rbuf[d, r - 1, unit(u), :].astype(F32)
+                sbuf[d, r, unit(u), :] = partial.astype(BF16)
+            sum_copy(r, d, u).start()
+
+    def send_back(u):
+        partial = product(u, y)
+        for d in range(2):
+            sum_copy(far - 1, d, u).wait_recv()
+            partial = partial + rbuf[d, far - 1, unit(u), :].astype(F32)
+        eo[unit(u), :] = partial.astype(BF16)
+        for place_j in range(2 * u, 2 * u + 2):
+            for i in range(n_x):
+                spot = place_j * n_x + i
+                dst = above(ORDER[place_j]) * n_x + i
+                if place_j == 0:
+
+                    @pl.when(x != i)
+                    def _():
+                        remote(eo.at[at(spot)], back.at[at(sp)], b_s, b_r, (dst, tp)).start()
+
+                else:
                     remote(eo.at[at(spot)], back.at[at(sp)], b_s, b_r, (dst, tp)).start()
 
-            else:
-                remote(eo.at[at(spot)], back.at[at(sp)], b_s, b_r, (dst, tp)).start()
-
-    lag = len(PAIRS) - 1
-    for t in range(-1, 2 * n_y + lag + 1):
-        for i, pair in enumerate(PAIRS):
-            step = t - i
-            for j in pair:
-                if step == -1:
-                    for k in range(j * n_x, (j + 1) * n_x):
-                        spot = rows.at[y, at(k)]
-                        pltpu.make_async_copy(spot, spot, d_r.at[k]).wait()
-                    ring_copy(0, j).start()
-                elif 0 <= step < n_y - 1:
-                    ring_copy(step, j).wait_recv()
-                    if step < n_y - 2:
-                        ring_copy(step + 1, j).start()
-        done = t - lag + 1
-        if 0 <= done <= early:
-            accumulate(source(done, 0), pl.ds(0, mid))
-            accumulate(source(done, STREAMS - 1), pl.ds(mid, mid))
-        for i, pair in enumerate(PAIRS):
-            step = t - i - (n_y - 2)
-            for j in pair:
-                if step == 0:
-                    finish(j)
-                if 0 <= step < n_y - 1:
-                    send_sum(step, j)
-                elif step == n_y - 1:
-                    send_back(j)
+    everything = pl.ds(0, slots)
+    for u in range(UNITS):
+        for k in range(2 * u * n_x, 2 * (u + 1) * n_x):
+            spot = rows.at[y, at(k)]
+            pltpu.make_async_copy(spot, spot, d_r.at[k]).wait()
+        for d in range(2):
+            hop(1, d, u).start()
+    accumulate(y, everything)
+
+    def pass_on(h, u):
+        for d in range(2):
+            hop_in(h, d, u).wait_recv()
+            hop(h + 1, d, u).start()
+
+    def through(u):
+        for d in range(2):
+            hop_in(far, d, u).wait_recv()
+        finish(u)
+        first_sums(u)
+
+    for h in range(1, far - 1):
+        for u in range(UNITS):
+            pass_on(h, u)
+        accumulate(chip(-h), everything)
+        accumulate(chip(h), everything)
+    behind = 3
+    for u in range(UNITS + behind):
+        if u < UNITS:
+            pass_on(far - 1, u)
+        if u >= behind:
+            through(u - behind)
+
+    for r in range(1, far):
+        for u in range(UNITS):
+            next_sums(r, u)
+    for u in range(UNITS):
+        send_back(u)
 
     stay = pltpu.make_async_copy(eo.at[at(x)], back.at[at(sp)], l_sem.at[5])
     stay.start()
@@ -403,7 +429,7 @@
     pltpu.make_async_copy(devs.at[many], devs.at[many], a_s).wait()
     pltpu.make_async_copy(gath.at[most], gath.at[most], d_s).wait()
     pltpu.make_async_copy(rows.at[many], rows.at[many], g_s).wait()
-    pltpu.make_async_copy(sbuf, sbuf, r_s).wait()
+    pltpu.make_async_copy(rows.at[many], rows.at[many], r_s).wait()
     pltpu.make_async_copy(eo.at[most], eo.at[most], b_s).wait()
 
 
@@ -442,15 +468,15 @@
             pltpu.VMEM((4, slots, ff), F32),
             pltpu.VMEM((slots, 128), F32),
             pltpu.VMEM((slots, 2 * ff), BF16),
-            pltpu.VMEM((n_y - 1, slots, cols), BF16),
-            pltpu.VMEM((n_y - 1, slots, cols), BF16),
+            pltpu.VMEM((2, n_y // 2, slots, cols), BF16),
+            pltpu.VMEM((2, n_y // 2, slots, cols), BF16),
             pltpu.VMEM((slots, cols), BF16),
             pltpu.VMEM((slots, cols), BF16),
             pltpu.VMEM((2, tok, cols // 2), F32),
             pltpu.VMEM((tok, cols // 2), F32),
             dma((6,)), dma((8,)), dma((8,)), dma((2,)), dma((2,)),
             dma, dma((n_y,)), dma, dma((n_y,)), dma, dma((n_y,)), dma, dma((n_y,)),
-            dma, dma((n_sp,)), dma, dma((n_y - 1, 8)), dma, dma((n_y - 1, 8)),
+            dma, dma((n_sp,)), dma, dma((2, n_y // 2, UNITS)), dma, dma((2, n_y // 2, UNITS)),
             dma, dma,
         ]
         return pl.pallas_call(

time: 119 us -> 97.4 us (0.82)
  Pallas kernels: 117 us -> 95.7 us
    pallas_call x1, Pallas kernels: 117 us -> 95.7 us  [local(): pl.pallas_call(functools.partial(layer, n_sp, n_y), out_shape=jax.ShapeDt...]
where the time goes in v3:
time: 97.4 us; the launch traced here: 97.1 us
  Pallas kernels  95.7 us (98%)
  local copies, waits for them, and re-layouts  1.47 us (2%)
    pallas_call x1, Pallas kernels, local(): pl.pallas_call(functools.partial(layer, n_sp, n_y), out_shape=jax.ShapeDt...  95.7 us

profile of v3, /device:TPU:1, one launch (start us, length us, event | category | flops | bytes accessed | tf_op | source)
XLA Modules:
  0.0 97.1 jit_solution(8112169949762544698)
XLA Ops:
  0.0 95.7 %shard_map.109 = bf16[256,128]{1,0:T(8,128)(2,1)} custom-call(bf16[64,256]{1,0:T(8,128)(2,1)} %bitcast.5, bf16[64,256]{1,0:T(8,128)(2,1)} %bitcast.6, bf16[31,64]{1,0:T(8,128)(2,1)} %taps.1, f32[1,64]{1,0:T(1,128)} %bitcast.9, bf16[64,2048]{1,0:T(8,128)(2,1)} %ow.1, bf16[256,2048]{1,0:T(8,128)(2,1)} %res.1, s32[2,256]{1,0:T(2,128)} %bitcast.7, ...), custom_call_target="tpu_custom_call" | custom-call | tf_op jit(solution)/shard_map/pallas_call | solution.py:482
  95.7 1.5 %copy.13 = bf16[256,128]{1,0:T(8,128)(2,1)} copy(bf16[256,128]{1,0:T(8,128)(2,1)} %shard_map.109) | data formatting | bytes 131072

commit v4 on v3

--- a/solution.py
+++ b/solution.py
@@ -29,12 +29,12 @@
 
 def layer(
     n_sp, n_y,
-    cv, cg, taps, gain, ow, res, ids, rw, eg, eu, ed,
+    cv_in, cg_in, taps_in, gain_in, ow, res, ids_in, rw_in, eg, eu, ed,
     out,
-    pk_own, pk_par, tg_own, tg_par, gext, stats, gains, gcol, devs, wc, resv, upd, ub, gs, wts,
-    gath, rows, wgu, wd, acc, ssq, hid, sbuf, rbuf, eo, back, xs, xr,
-    l_sem, sw_s, sw_r, h_s, h_r, w_s, w_r, st_s, st_r, a_s, a_r, gn_s, gn_r, d_s, d_r, g_s, g_r,
-    r_s, r_r, b_s, b_r,
+    cv, cg, taps, gain, ids, rw, pk_own, pk_par, tg_own, tg_par, gext, stats, gcol, devs, wc, resv, upd, updx, ups, ub, gs, takes, wts,
+    first_rows, gath, rows, wgu, wd, acc, ssq, hid, sbuf, rbuf, eo, back,
+    l_sem, sw_s, sw_r, h_s, h_r, w_s, w_r, st_s, st_r, a_s, a_r, x_s, x_r, c_s, c_r, d_s, d_r, g_s, g_r,
+    r_s, r_r, b_s, b_r, tok_sem,
 ):
     sp, tp = lax.axis_index("sp"), lax.axis_index("tp")
     y, c = tp // 2, tp % 2
@@ -56,48 +56,76 @@
     def column(k):
         return (sp, lax.rem(y + k, n_y) * 2 + c)
 
+    def chip(k):
+        return lax.rem(y + n_y + k, n_y)
+
     def remote(src, dst, s, r, dev):
         return pltpu.make_async_remote_copy(
             src_ref=src, dst_ref=dst, send_sem=s, recv_sem=r, device_id=dev, device_id_type=MESH
         )
 
+    barrier = pltpu.get_barrier_semaphore()
+
+    def greet(dev):
+        pl.semaphore_signal(barrier, inc=1, device_id=dev, device_id_type=MESH)
+
+    nxt = lax.rem(sp + 1, n_sp)
+    prv = lax.rem(sp + n_sp - 1, n_sp)
+    z_next = (lax.rem(z + 1, STREAMS) * n_x + x, tp)
+    z_prev = (lax.rem(z + STREAMS - 1, STREAMS) * n_x + x, tp)
+    near = [column(k) for k in range(n_y - 1, 0, -1)]
+    for i in range(1, n_x):
+        side = z * n_x + lax.rem(x + i, n_x)
+        near += [(side, tp), (side, y * 2 + other)]
+    near += [z_next, z_prev, partner]
+    for dev in near:
+        greet(dev)
+
+    @pl.when(sp < n_sp - 1)
+    def _():
+        greet((nxt, tp))
+        greet((nxt, y * 2 + other))
+
+    @pl.when(sp > 0)
+    def _():
+        greet((prv, tp))
+        greet((prv, y * 2 + other))
+
+    ends = jnp.where(sp > 0, 2, 0) + jnp.where(sp < n_sp - 1, 2, 0)
+
+    def token(r):
+        for dev in (z_next, z_prev):
+            pl.semaphore_signal(tok_sem.at[r], inc=1, device_id=dev, device_id_type=MESH)
+
     my_cols = pl.ds(pl.multiple_of(y * cols, cols), cols)
     my_half = pl.ds(pl.multiple_of(c * half, half), half)
     own_rows = pl.ds(pl.multiple_of(c * ch, ch), ch)
+    half_ch = ch // 2
+    pair_x = sp + 1 - 2 * (x % 2)
+    pair_rows = pl.ds(pl.multiple_of((x % 2) * half_ch, half_ch), half_ch)
+    own_pair = pl.ds(pl.multiple_of(c * ch + (x % 2) * half_ch, half_ch), half_ch)
+    small = [
+        pltpu.make_async_copy(src, dst, l_sem.at[6 + i])
+        for i, (src, dst) in enumerate(
+            ((cv_in, cv), (cg_in, cg), (taps_in, taps), (gain_in, gain), (ids_in, ids), (rw_in, rw))
+        )
+    ]
     loads = [
         pltpu.make_async_copy(res.at[my_half, my_cols], resv, l_sem.at[0]),
         pltpu.make_async_copy(eg.at[0], wgu.at[0], l_sem.at[1]),
         pltpu.make_async_copy(eu.at[0], wgu.at[2], l_sem.at[2]),
         pltpu.make_async_copy(ed.at[0], wd.at[pl.ds(0, ff)], l_sem.at[3]),
-        pltpu.make_async_copy(ow.at[:, my_cols], wc.at[y, own_rows], l_sem.at[4]),
+        pltpu.make_async_copy(ow.at[pair_rows, my_cols], wc.at[y, own_pair], l_sem.at[4]),
     ]
-    for load in loads:
+    for load in small + loads:
         load.start()
-
-    barrier = pltpu.get_barrier_semaphore()
-
-    def greet(dev):
-        pl.semaphore_signal(barrier, inc=1, device_id=dev, device_id_type=MESH)
-
-    nxt = lax.rem(sp + 1, n_sp)
-    prv = lax.rem(sp + n_sp - 1, n_sp)
-
-    @pl.loop(1, n_sp)
-    def _(k):
-        greet((lax.rem(sp + k, n_sp), tp))
-
-    @pl.loop(1, n_y)
-    def _(k):
-        greet(column(k))
-
-    greet((nxt, y * 2 + other))
-    greet((prv, y * 2 + other))
-    greet(partner)
 
     lane = iota((ch, wide), 1)
     chan = iota((ch, wide), 0)
     put_low = (lane == chan).astype(BF16)
     put_high = (lane == chan + ch).astype(BF16)
+    for load in small[0:4]:
+        load.wait()
     pk_own[pl.ds(HALO, tok), :] = (
         matmul_t(cv[...], put_low) + matmul_t(cg[...], put_high)
     ).astype(BF16)
@@ -108,19 +136,7 @@
         jnp.broadcast_to(gain[...], (8, ch)), put_low.astype(F32), lax.Precision.HIGHEST
     )[0:1]
 
-    expert = iota((128, tok), 0)
-    id0, id1 = ids[0:1, :], ids[1:2, :]
-    hot0, hot1 = (id0 == expert).astype(F32), (id1 == expert).astype(F32)
-    before = (iota((tok, tok), 0) < iota((tok, tok), 1)).astype(BF16)
-    earlier = matmul((hot0 + hot1).astype(BF16), before)
-    place = iota((slots, tok), 0)
-    for k, (ident, hot) in enumerate(((id0, hot0), (id1, hot1))):
-        rank = jnp.sum(earlier * hot, axis=0, keepdims=True).astype(jnp.int32) - c * per
-        slot = jnp.where((rank >= 0) & (rank < per), ident * per + rank, -1)
-        gs[k] = jnp.where(place == slot, 1.0, 0.0).astype(BF16)
-        wts[k] = jnp.transpose(jnp.broadcast_to(rw[k : k + 1, :], (128, tok)))
-
-    pl.semaphore_wait(barrier, 3 + (n_y - 1) + (n_sp - 1))
+    pl.semaphore_wait(barrier, len(near) + ends)
 
     body = pl.ds(HALO, tok)
     head = pl.ds(0, HALO)
@@ -129,26 +145,46 @@
         remote(pk_own.at[tail], pk_own.at[head], h_s.at[0], h_r.at[0], (nxt, tp)),
         remote(pk_own.at[tail], pk_par.at[head], h_s.at[1], h_r.at[1], (nxt, y * 2 + other)),
     ]
-    for copy in halo:
-        copy.start()
+
+    @pl.when(sp < n_sp - 1)
+    def _():
+        for copy in halo:
+            copy.start()
+
+    @pl.when(sp == 0)
+    def _():
+        pk_own[head, :] = jnp.zeros((HALO, wide), BF16)
+        pk_par[head, :] = jnp.zeros((HALO, wide), BF16)
+
     swap_tg = remote(tg_own, tg_par, sw_s.at[1], sw_r.at[1], partner)
     swap_pk = remote(pk_own.at[body], pk_par.at[body], sw_s.at[0], sw_r.at[0], partner)
     swap_tg.start()
     swap_pk.start()
 
-    @pl.loop(1, n_y)
-    def _(k):
-        dst_chip = lax.rem(y + k, n_y)
-        far_cols = pl.ds(pl.multiple_of(dst_chip * cols, cols), cols)
-        remote(ow.at[:, far_cols], wc.at[y, own_rows], w_s, w_r.at[y], column(k)).start()
-
+    outward = (1, n_y - 1, 2, n_y - 2, 3, n_y - 3, far)
+    for k in outward:
+        far_cols = pl.ds(pl.multiple_of(chip(k) * cols, cols), cols)
+        remote(ow.at[pair_rows, far_cols], wc.at[y, own_pair], w_s, w_r.at[y], column(k)).start()
+
+    token(0)
     swap_w = [
         remote(eg.at[0], wgu.at[1], sw_s.at[2], sw_r.at[2], partner),
         remote(eu.at[0], wgu.at[3], sw_s.at[3], sw_r.at[3], partner),
         remote(ed.at[0], wd.at[pl.ds(ff, ff)], sw_s.at[4], sw_r.at[4], partner),
     ]
-    for copy in swap_w:
-        copy.start()
+    for load in small[4:6]:
+        load.wait()
+    expert = iota((128, tok), 0)
+    id0, id1 = ids[0:1, :], ids[1:2, :]
+    hot0, hot1 = (id0 == expert).astype(F32), (id1 == expert).astype(F32)
+    before = (iota((tok, tok), 0) < iota((tok, tok), 1)).astype(BF16)
+    earlier = matmul((hot0 + hot1).astype(BF16), before)
+    place = iota((slots, tok), 0) + c * slots
+    slot_rows = []
+    for ident, hot in ((id0, hot0), (id1, hot1)):
+        rank = jnp.sum(earlier * hot, axis=0, keepdims=True).astype(jnp.int32)
+        slot_rows.append(jnp.where(rank < per, 0, slots - per) + ident * per + rank)
+    gs[...] = jnp.where((place == slot_rows[0]) | (place == slot_rows[1]), 1.0, 0.0).astype(BF16)
 
     lane2, chan2 = iota((wide, wide), 1), iota((wide, wide), 0)
 
@@ -172,9 +208,19 @@
         remote(buf.at[origin], buf.at[origin], s, r.at[origin], column(k)).wait_recv()
         return origin
 
+    def tokens(r):
+        pl.semaphore_wait(tok_sem.at[r], 2)
+        if r < STREAMS // 2 - 1:
+            token(r + 1)
+
+    tokens(0)
     swap_pk.wait_recv()
-    for copy in halo:
-        copy.wait_recv()
+
+    @pl.when(sp > 0)
+    def _():
+        for copy in halo:
+            copy.wait_recv()
+
     span = pl.ds(pl.multiple_of(c * half, half), half + HALO)
     mine, theirs = pk_own[span, :], pk_par[span, :]
     value = matmul(mine, pick(0, c)) + matmul(theirs, pick(0, other))
@@ -191,28 +237,46 @@
     turned = turned - mean
     spread = jnp.sum(turned * turned, axis=0, keepdims=True) / wide
     devs[y] = turned.astype(BF16)
-    stats[y] = jnp.where(iota((8, half), 0) == 0, mean, spread)
-    gains[y] = jnp.broadcast_to(tg[n_taps : n_taps + 1, :], (8, wide))
+    line = iota((8, half), 0)
+    note = jnp.where(line == 1, spread, jnp.broadcast_to(tg[n_taps : n_taps + 1, :], (8, half)))
+    stats[y] = jnp.where(line == 0, mean, note)
     everywhere(stats, st_s, st_r)
-    everywhere(gains, gn_s, gn_r)
-    everywhere(devs, a_s, a_r)
-
-    loads[4].wait()
-
-    @pl.loop(1, n_y)
-    def _(k):
+
+    def tell(origin, k, r):
+        remote(devs.at[origin], devs.at[origin], a_s, r, column(k)).start()
+
+    for k in (2, n_y - 2, 1, n_y - 1):
+        tell(y, k, a_r.at[y])
+    tokens(1)
+
+    def hear(k):
         origin = lax.rem(y + k, n_y)
-        remote(
-            wc.at[origin, own_rows], wc.at[origin, own_rows], w_s, w_r.at[origin], column(k)
-        ).wait_recv()
-
-    swap_wc = remote(wc.at[:, own_rows], wc.at[:, own_rows], sw_s.at[5], sw_r.at[5], partner)
-    swap_wc.start()
+        remote(devs.at[origin], devs.at[origin], a_s, a_r.at[origin], partner).wait_recv()
+        return origin
+
+    def share(k):
+        block = wc.at[chip(k), own_pair]
+        if k == 0:
+            loads[4].wait()
+        else:
+            remote(block, block, w_s, w_r.at[chip(k)], partner).wait_recv()
+        remote(block, block, x_s, x_r.at[chip(k)], (pair_x, tp)).start()
+
+    for k in (0,) + outward[0:4]:
+        share(k)
+    for k, on in ((n_y - 2, 1), (2, n_y - 1)):
+        origin = hear(k)
+        tell(origin, on, a_r.at[origin])
+        piece_of = devs.at[origin, pl.ds(0 if on == 1 else ch, ch)]
+        sem = a_r.at[origin] if on == 1 else a_r.at[n_y]
+        remote(piece_of, piece_of, a_s, sem, column(2 if on == 1 else n_y - 2)).start()
+    for k in outward[4:]:
+        share(k)
+    tokens(2)
 
     @pl.loop(1, n_y)
     def _(k):
         arrived(stats, st_s, st_r, k)
-        arrived(gains, gn_s, gn_r, k)
 
     average = stats[0, 0:1, :]
     for o in range(1, n_y):
@@ -224,7 +288,7 @@
         variance = variance + (stats[o, 1:2, :] + gap * gap)
     scale = lax.rsqrt(variance / n_y + 1e-05)
     for o in range(n_y):
-        gcol[o] = jnp.transpose(jnp.broadcast_to(gains[o, 0:1, :], (half, wide))) * scale
+        gcol[o] = jnp.transpose(jnp.broadcast_to(stats[o, 2:3, :], (half, wide))) * scale
 
     def mixed(origin):
         shift = stats[origin, 0:1, :] - average
@@ -232,18 +296,47 @@
         activated = (normed / (1.0 + jnp.exp(-normed))).astype(BF16)
         return matmul_t(activated, wc[origin])
 
+    for k in (0,) + outward:
+        block = wc.at[chip(k), own_pair]
+        remote(block, block, x_s, x_r.at[chip(k)], partner).wait_recv()
+        block = wc.at[chip(k), own_rows]
+        remote(block, block, c_s, c_r.at[chip(k)], partner).start()
+
+    def whole(k):
+        block = wc.at[chip(k), own_rows]
+        remote(block, block, c_s, c_r.at[chip(k)], partner).wait_recv()
+        return chip(k)
+
     loads[0].wait()
-    swap_wc.wait_recv()
+    whole(0)
     upd[...] = resv[...].astype(F32) + mixed(y)
-    for k in (1, 7, 2, 6, 3, 5, 4) if n_y == 8 else range(1, n_y):
-        upd[...] += mixed(arrived(devs, a_s, a_r, k))
+    for k in outward[0:6]:
+        if k not in (2, n_y - 2):
+            hear(k)
+        upd[...] += mixed(whole(k))
+    last_half = devs.at[chip(far), pl.ds(0, ch)]
+    for sem in (a_r.at[chip(far)], a_r.at[n_y]):
+        remote(last_half, last_half, a_s, sem, partner).wait_recv()
+    upd[...] += mixed(whole(far))
 
     ub[my_half, :] = upd[...].astype(BF16)
     swap_ub = remote(ub.at[my_half], ub.at[my_half], sw_s.at[6], sw_r.at[6], partner)
     swap_ub.start()
+    narrow = cols // 2
+    for t in range(2):
+
+        @pl.when(c == t)
+        def _():
+            updx[t] = upd[:, t * narrow : (t + 1) * narrow]
+            ups[...] = upd[:, (1 - t) * narrow : (2 - t) * narrow]
+
+    swap_upd = remote(ups, updx.at[c], sw_s.at[7], sw_r.at[7], partner)
+    swap_upd.start()
+    for copy in swap_w:
+        copy.start()
     swap_ub.wait_recv()
 
-    gath[...] = matmul(gs[0] + gs[1], ub[...]).astype(BF16)
+    tokens(3)
 
     def at(k):
         return pl.ds(pl.multiple_of(k * per, per), per)
@@ -254,20 +347,35 @@
     def above(j):
         return lax.rem(z + j, STREAMS)
 
+    block_z = n_x * per
     for place_j, j in enumerate(ORDER):
         spot = place_j * n_x + x
+        to_z = pl.ds(pl.multiple_of(below(j) * block_z, block_z), block_z)
+        if place_j < 2:
+            picked = matmul(gs[to_z, :], ub[...]).astype(BF16)
+            first_rows[pl.ds(place_j * block_z, block_z), :] = picked
+        elif place_j == 2:
+            gath[...] = matmul(gs[...], ub[...]).astype(BF16)
         for i in range(n_x):
             dst = below(j) * n_x + lax.rem(x + i, n_x)
+            if place_j < 2:
+                start_at = place_j * block_z + lax.rem(x + i, n_x) * per
+                src = first_rows.at[pl.ds(pl.multiple_of(start_at, per), per)]
+            else:
+                src = gath.at[at(dst)]
             if i == 0 and j == 0:
-                keep = pltpu.make_async_copy(gath.at[at(dst)], rows.at[y, at(spot)], d_r.at[spot])
+                keep = pltpu.make_async_copy(src, rows.at[y, at(spot)], d_r.at[spot])
                 keep.start()
             else:
-                remote(gath.at[at(dst)], rows.at[y, at(spot)], d_s, d_r.at[spot], (dst, tp)).start()
-
-    for load in loads[1:4]:
-        load.wait()
-    for copy in swap_w:
-        copy.wait_recv()
+                remote(src, rows.at[y, at(spot)], d_s, d_r.at[spot], (dst, tp)).start()
+
+    for k in range(2):
+        wts[k] = jnp.transpose(jnp.broadcast_to(rw[k : k + 1, :], (128, tok)))
+        slot = jnp.transpose(jnp.broadcast_to(slot_rows[k].astype(F32), (128, tok)))
+        for m in range(2 * slots // 128):
+            here = (iota((tok, 128), 1) + m * 128).astype(F32)
+            takes[k, :, m * 128 : (m + 1) * 128] = jnp.where(slot == here, 1.0, 0.0).astype(BF16)
+
     acc[...] = jnp.zeros_like(acc)
     ssq[...] = jnp.zeros_like(ssq)
 
@@ -276,9 +384,6 @@
 
     def piece(u, d):
         return pl.ds(u * size + d * (size // 2), size // 2)
-
-    def chip(k):
-        return lax.rem(y + n_y + k, n_y)
 
     def hop(h, d, u):
         origin = chip(1 - h if d == 0 else h - 1)
@@ -347,24 +452,30 @@
                 sbuf[d, r, unit(u), :] = partial.astype(BF16)
             sum_copy(r, d, u).start()
 
+    came = pl.ds(pl.multiple_of(c * slots + sp * per, per), per)
+
     def send_back(u):
         partial = product(u, y)
         for d in range(2):
             sum_copy(far - 1, d, u).wait_recv()
             partial = partial + rbuf[d, far - 1, unit(u), :].astype(F32)
-        eo[unit(u), :] = partial.astype(BF16)
+        for t in range(2):
+            eo[t, unit(u), :] = partial[:, t * narrow : (t + 1) * narrow].astype(BF16)
         for place_j in range(2 * u, 2 * u + 2):
             for i in range(n_x):
                 spot = place_j * n_x + i
                 dst = above(ORDER[place_j]) * n_x + i
+
+                def send(t):
+                    remote(eo.at[t, at(spot)], back.at[came], b_s, b_r, (dst, y * 2 + t)).start()
+
+                send_far = functools.partial(send, other)
+                send_near = functools.partial(send, c)
+                send_far()
                 if place_j == 0:
-
-                    @pl.when(x != i)
-                    def _():
-                        remote(eo.at[at(spot)], back.at[at(sp)], b_s, b_r, (dst, tp)).start()
-
+                    pl.when(x != i)(send_near)
                 else:
-                    remote(eo.at[at(spot)], back.at[at(sp)], b_s, b_r, (dst, tp)).start()
+                    send_near()
 
     everything = pl.ds(0, slots)
     for u in range(UNITS):
@@ -373,6 +484,11 @@
             pltpu.make_async_copy(spot, spot, d_r.at[k]).wait()
         for d in range(2):
             hop(1, d, u).start()
+
+    for load in loads[1:4]:
+        load.wait()
+    for copy in swap_w:
+        copy.wait_recv()
     accumulate(y, everything)
 
     def pass_on(h, u):
@@ -404,33 +520,36 @@
     for u in range(UNITS):
         send_back(u)
 
-    stay = pltpu.make_async_copy(eo.at[at(x)], back.at[at(sp)], l_sem.at[5])
+    stay = pltpu.make_async_copy(eo.at[c, at(x)], back.at[came], l_sem.at[5])
     stay.start()
     stay.wait()
-    most = pl.ds(0, slots - per)
+    swap_upd.wait_recv()
+    most = pl.ds(0, 2 * slots - per)
     pltpu.make_async_copy(back.at[most], back.at[most], b_r).wait()
 
-    first, second = matmul_t(gs[0], back[...]), matmul_t(gs[1], back[...])
-    for i in range(2):
-        lanes = slice(i * (cols // 2), (i + 1) * (cols // 2))
-        xs[i] = wts[0] * first[:, lanes] + wts[1] * second[:, lanes]
-        xs[i, my_half, :] += upd[:, lanes]
-    last = remote(xs.at[other], xr, sw_s.at[7], sw_r.at[7], partner)
-    last.start()
-    last.wait_recv()
-    out[...] = (xs[c] + xr[...]).astype(BF16)
-
-    for copy in halo + swap_w + [swap_pk, swap_tg, swap_wc, swap_ub, last]:
+    combined = wts[0] * matmul(takes[0], back[...]) + wts[1] * matmul(takes[1], back[...])
+    for t in range(2):
+        block = slice(t * half, (t + 1) * half)
+        out[block, :] = (updx[t] + combined[block]).astype(BF16)
+
+    @pl.when(sp < n_sp - 1)
+    def _():
+        for copy in halo:
+            copy.wait_send()
+
+    for copy in swap_w + [swap_pk, swap_tg, swap_ub, swap_upd]:
         copy.wait_send()
+    pltpu.make_async_copy(wc.at[:, own_pair], wc.at[:, own_pair], x_s).wait()
+    pltpu.make_async_copy(wc.at[:, own_rows], wc.at[:, own_rows], c_s).wait()
     many = pl.ds(0, n_y - 1)
-    pltpu.make_async_copy(wc.at[many, own_rows], wc.at[many, own_rows], w_s).wait()
+    pltpu.make_async_copy(wc.at[many, own_pair], wc.at[many, own_pair], w_s).wait()
     pltpu.make_async_copy(stats.at[many], stats.at[many], st_s).wait()
-    pltpu.make_async_copy(gains.at[many], gains.at[many], gn_s).wait()
     pltpu.make_async_copy(devs.at[many], devs.at[many], a_s).wait()
-    pltpu.make_async_copy(gath.at[most], gath.at[most], d_s).wait()
+    fewer = pl.ds(0, slots - per)
+    pltpu.make_async_copy(gath.at[fewer], gath.at[fewer], d_s).wait()
     pltpu.make_async_copy(rows.at[many], rows.at[many], g_s).wait()
     pltpu.make_async_copy(rows.at[many], rows.at[many], r_s).wait()
-    pltpu.make_async_copy(eo.at[most], eo.at[most], b_s).wait()
+    pltpu.make_async_copy(back.at[most], back.at[most], b_s).wait()
 
 
 def solution(mesh):
@@ -446,21 +565,30 @@
         vm, hbm = pl.BlockSpec(memory_space=pltpu.VMEM), pl.BlockSpec(memory_space=pl.ANY)
         dma = pltpu.SemaphoreType.DMA
         scratch = [
+            pltpu.VMEM((ch, tok), BF16),
+            pltpu.VMEM((ch, tok), BF16),
+            pltpu.VMEM(taps.shape, BF16),
+            pltpu.VMEM((1, ch), F32),
+            pltpu.VMEM(ids.shape[::-1], jnp.int32),
+            pltpu.VMEM(rw.shape[::-1], F32),
             pltpu.VMEM((HALO + tok, 2 * ch), BF16),
             pltpu.VMEM((HALO + tok, 2 * ch), BF16),
             pltpu.VMEM((40, 2 * ch), F32),
             pltpu.VMEM((40, 2 * ch), F32),
             pltpu.VMEM((HALO + half, 2 * ch), F32),
             pltpu.VMEM((n_y, 8, half), F32),
-            pltpu.VMEM((n_y, 8, 2 * ch), F32),
             pltpu.VMEM((n_y, 2 * ch, half), F32),
             pltpu.VMEM((n_y, 2 * ch, half), BF16),
             pltpu.VMEM((n_y, 2 * ch, cols), BF16),
             pltpu.VMEM((half, cols), BF16),
             pltpu.VMEM((half, cols), F32),
+            pltpu.VMEM((2, half, cols // 2), F32),
+            pltpu.VMEM((half, cols // 2), F32),
             pltpu.VMEM((tok, cols), BF16),
-            pltpu.VMEM((2, slots, tok), BF16),
+            pltpu.VMEM((slots, tok), BF16),
+            pltpu.VMEM((2, tok, 2 * slots), BF16),
             pltpu.VMEM((2, tok, 128), F32),
+            pltpu.VMEM((slots // UNITS, cols), BF16),
             pltpu.VMEM((slots, cols), BF16),
             pltpu.VMEM((n_y, slots, cols), BF16),
             pltpu.VMEM((4, width, ff), BF16),
@@ -470,19 +598,19 @@
             pltpu.VMEM((slots, 2 * ff), BF16),
             pltpu.VMEM((2, n_y // 2, slots, cols), BF16),
             pltpu.VMEM((2, n_y // 2, slots, cols), BF16),
-            pltpu.VMEM((slots, cols), BF16),
-            pltpu.VMEM((slots, cols), BF16),
-            pltpu.VMEM((2, tok, cols // 2), F32),
-            pltpu.VMEM((tok, cols // 2), F32),
-            dma((6,)), dma((8,)), dma((8,)), dma((2,)), dma((2,)),
-            dma, dma((n_y,)), dma, dma((n_y,)), dma, dma((n_y,)), dma, dma((n_y,)),
+            pltpu.VMEM((2, slots, cols // 2), BF16),
+            pltpu.VMEM((2 * slots, cols // 2), BF16),
+            dma((12,)), dma((8,)), dma((8,)), dma((2,)), dma((2,)),
+            dma, dma((n_y,)), dma, dma((n_y,)), dma, dma((n_y + 1,)),
+            dma, dma((n_y,)), dma, dma((n_y,)),
             dma, dma((n_sp,)), dma, dma((2, n_y // 2, UNITS)), dma, dma((2, n_y // 2, UNITS)),
             dma, dma,
+            pltpu.SemaphoreType.REGULAR((STREAMS // 2,)),
         ]
         return pl.pallas_call(
             functools.partial(layer, n_sp, n_y),
             out_shape=jax.ShapeDtypeStruct((tok, cols // 2), BF16),
-            in_specs=[vm, vm, vm, vm, hbm, hbm, vm, vm, hbm, hbm, hbm],
+            in_specs=[hbm] * 11,
             out_specs=vm,
             scratch_shapes=scratch,
             compiler_params=pltpu.CompilerParams(

time: 97.4 us -> 89.1 us (0.915)
  Pallas kernels: 95.7 us -> 87.5 us
    pallas_call x1, Pallas kernels: 95.7 us -> 87.5 us  [local(): pl.pallas_call(functools.partial(layer, n_sp, n_y), out_shape=jax.ShapeDt...]
where the time goes in v4:
time: 89.1 us; the launch traced here: 89 us
  Pallas kernels  87.5 us (98%)
  local copies, waits for them, and re-layouts  1.47 us (2%)
    pallas_call x1, Pallas kernels, local(): pl.pallas_call(functools.partial(layer, n_sp, n_y), out_shape=jax.ShapeDt...  87.5 us

profile of v4, /device:TPU:1, one launch (start us, length us, event | category | flops | bytes accessed | tf_op | source)
XLA Modules:
  0.0 89.0 jit_solution(10964940076816704319)
XLA Ops:
  0.0 87.5 %shard_map.109 = bf16[256,128]{1,0:T(8,128)(2,1)} custom-call(bf16[64,256]{1,0:T(8,128)(2,1)} %bitcast.5, bf16[64,256]{1,0:T(8,128)(2,1)} %bitcast.6, bf16[31,64]{1,0:T(8,128)(2,1)} %taps_in.1, f32[1,64]{1,0:T(1,128)} %bitcast.9, bf16[64,2048]{1,0:T(8,128)(2,1)} %ow.1, bf16[256,2048]{1,0:T(8,128)(2,1)} %res.1, s32[2,256]{1,0:T(2,128)} %bitcast.7, ...), custom_call_target="tpu_custom_call" | custom-call | tf_op jit(solution)/shard_map/pallas_call | solution.py:610
  87.5 1.5 %copy.13 = bf16[256,128]{1,0:T(8,128)(2,1)} copy(bf16[256,128]{1,0:T(8,128)(2,1)} %shard_map.109) | data formatting | bytes 131072

commit v5 on v4

--- a/solution.py
+++ b/solution.py
@@ -12,7 +12,8 @@
 HALO = 32
 STREAMS = 8
 UNITS = 4
-ORDER = (0, 7, 1, 6, 2, 5, 3, 4)
+ORDER = (0, 7, 3, 4, 2, 5, 1, 6)
+SENDING = (0, 7, 4, 3, 5, 2, 6, 1)
 
 
 def iota(shape, dim):
@@ -31,7 +32,7 @@
     n_sp, n_y,
     cv_in, cg_in, taps_in, gain_in, ow, res, ids_in, rw_in, eg, eu, ed,
     out,
-    cv, cg, taps, gain, ids, rw, pk_own, pk_par, tg_own, tg_par, gext, stats, gcol, devs, wc, resv, upd, updx, ups, ub, gs, takes, wts,
+    cv, cg, taps, gain, ids, rw, owv, pk_own, pk_par, tg_own, tg_par, gext, stats, gcol, devs, wc, resv, upd, updx, ups, ub, gs, takes, wts,
     first_rows, gath, rows, wgu, wd, acc, ssq, hid, sbuf, rbuf, eo, back,
     l_sem, sw_s, sw_r, h_s, h_r, w_s, w_r, st_s, st_r, a_s, a_r, x_s, x_r, c_s, c_r, d_s, d_r, g_s, g_r,
     r_s, r_r, b_s, b_r, tok_sem,
@@ -115,9 +116,9 @@
         pltpu.make_async_copy(eg.at[0], wgu.at[0], l_sem.at[1]),
         pltpu.make_async_copy(eu.at[0], wgu.at[2], l_sem.at[2]),
         pltpu.make_async_copy(ed.at[0], wd.at[pl.ds(0, ff)], l_sem.at[3]),
-        pltpu.make_async_copy(ow.at[pair_rows, my_cols], wc.at[y, own_pair], l_sem.at[4]),
     ]
-    for load in small + loads:
+    bring_ow = pltpu.make_async_copy(ow.at[pair_rows], owv, l_sem.at[12])
+    for load in small + [bring_ow] + loads:
         load.start()
 
     lane = iota((ch, wide), 1)
@@ -162,9 +163,13 @@
     swap_pk.start()
 
     outward = (1, n_y - 1, 2, n_y - 2, 3, n_y - 3, far)
-    for k in outward:
+    bring_ow.wait()
+    keep_w = pltpu.make_async_copy(owv.at[:, my_cols], wc.at[y, own_pair], l_sem.at[4])
+    keep_w.start()
+    inward = (far, 3, n_y - 3, 2, n_y - 2, 1, n_y - 1)
+    for k in inward:
         far_cols = pl.ds(pl.multiple_of(chip(k) * cols, cols), cols)
-        remote(ow.at[pair_rows, far_cols], wc.at[y, own_pair], w_s, w_r.at[y], column(k)).start()
+        remote(owv.at[:, far_cols], wc.at[y, own_pair], w_s, w_r.at[y], column(k)).start()
 
     token(0)
     swap_w = [
@@ -257,12 +262,12 @@
     def share(k):
         block = wc.at[chip(k), own_pair]
         if k == 0:
-            loads[4].wait()
+            keep_w.wait()
         else:
             remote(block, block, w_s, w_r.at[chip(k)], partner).wait_recv()
         remote(block, block, x_s, x_r.at[chip(k)], (pair_x, tp)).start()
 
-    for k in (0,) + outward[0:4]:
+    for k in (0, 1, n_y - 1, 2, n_y - 2, 3, n_y - 3, far):
         share(k)
     for k, on in ((n_y - 2, 1), (2, n_y - 1)):
         origin = hear(k)
@@ -270,8 +275,6 @@
         piece_of = devs.at[origin, pl.ds(0 if on == 1 else ch, ch)]
         sem = a_r.at[origin] if on == 1 else a_r.at[n_y]
         remote(piece_of, piece_of, a_s, sem, column(2 if on == 1 else n_y - 2)).start()
-    for k in outward[4:]:
-        share(k)
     tokens(2)
 
     @pl.loop(1, n_y)
@@ -348,13 +351,14 @@
         return lax.rem(z + j, STREAMS)
 
     block_z = n_x * per
-    for place_j, j in enumerate(ORDER):
+    for turn_j, j in enumerate(SENDING):
+        place_j = ORDER.index(j)
         spot = place_j * n_x + x
         to_z = pl.ds(pl.multiple_of(below(j) * block_z, block_z), block_z)
         if place_j < 2:
             picked = matmul(gs[to_z, :], ub[...]).astype(BF16)
             first_rows[pl.ds(place_j * block_z, block_z), :] = picked
-        elif place_j == 2:
+        elif turn_j == 2:
             gath[...] = matmul(gs[...], ub[...]).astype(BF16)
         for i in range(n_x):
             dst = below(j) * n_x + lax.rem(x + i, n_x)
@@ -414,8 +418,7 @@
 
     def finish(u):
         block = unit(u)
-        for origin in (chip(1 - far), chip(far - 1), chip(far)):
-            accumulate(origin, block)
+        accumulate(chip(far), block)
         rms = lax.rsqrt(jnp.sum(ssq[block, :], axis=1, keepdims=True) / width + 1e-06)
         for i in range(2):
             g = acc[i, block, :] * rms
@@ -511,6 +514,8 @@
     for u in range(UNITS + behind):
         if u < UNITS:
             pass_on(far - 1, u)
+            accumulate(chip(1 - far), unit(u))
+            accumulate(chip(far - 1), unit(u))
         if u >= behind:
             through(u - behind)
 
@@ -571,6 +576,7 @@
             pltpu.VMEM((1, ch), F32),
             pltpu.VMEM(ids.shape[::-1], jnp.int32),
             pltpu.VMEM(rw.shape[::-1], F32),
+            pltpu.VMEM((ch // 2, width), BF16),
             pltpu.VMEM((HALO + tok, 2 * ch), BF16),
             pltpu.VMEM((HALO + tok, 2 * ch), BF16),
             pltpu.VMEM((40, 2 * ch), F32),
@@ -600,7 +606,7 @@
             pltpu.VMEM((2, n_y // 2, slots, cols), BF16),
             pltpu.VMEM((2, slots, cols // 2), BF16),
             pltpu.VMEM((2 * slots, cols // 2), BF16),
-            dma((12,)), dma((8,)), dma((8,)), dma((2,)), dma((2,)),
+            dma((13,)), dma((8,)), dma((8,)), dma((2,)), dma((2,)),
             dma, dma((n_y,)), dma, dma((n_y,)), dma, dma((n_y + 1,)),
             dma, dma((n_y,)), dma, dma((n_y,)),
             dma, dma((n_sp,)), dma, dma((2, n_y // 2, UNITS)), dma, dma((2, n_y // 2, UNITS)),

time: 89.1 us -> 88.4 us (level)
  no operation moved by 1% of the time
where the time goes in v5:
time: 88.4 us; the launch traced here: 88.2 us
  Pallas kernels  86.7 us (98%)
  local copies, waits for them, and re-layouts  1.47 us (2%)
    pallas_call x1, Pallas kernels, local(): pl.pallas_call(functools.partial(layer, n_sp, n_y), out_shape=jax.ShapeDt...  86.7 us

profile of v5, /device:TPU:1, one launch (start us, length us, event | category | flops | bytes accessed | tf_op | source)
XLA Modules:
  0.0 88.2 jit_solution(3291919754535168489)
XLA Ops:
  0.0 86.7 %shard_map.109 = bf16[256,128]{1,0:T(8,128)(2,1)} custom-call(bf16[64,256]{1,0:T(8,128)(2,1)} %bitcast.5, bf16[64,256]{1,0:T(8,128)(2,1)} %bitcast.6, bf16[31,64]{1,0:T(8,128)(2,1)} %taps_in.1, f32[1,64]{1,0:T(1,128)} %bitcast.9, bf16[64,2048]{1,0:T(8,128)(2,1)} %ow.1, bf16[256,2048]{1,0:T(8,128)(2,1)} %res.1, s32[2,256]{1,0:T(2,128)} %bitcast.7, ...), custom_call_target="tpu_custom_call" | custom-call | tf_op jit(solution)/shard_map/pallas_call | solution.py:616
  86.7 1.5 %copy.13 = bf16[256,128]{1,0:T(8,128)(2,1)} copy(bf16[256,128]{1,0:T(8,128)(2,1)} %shard_map.109) | data formatting | bytes 131072

commit v6 on v5

--- a/solution.py
+++ b/solution.py
@@ -335,8 +335,6 @@
 
     swap_upd = remote(ups, updx.at[c], sw_s.at[7], sw_r.at[7], partner)
     swap_upd.start()
-    for copy in swap_w:
-        copy.start()
     swap_ub.wait_recv()
 
     tokens(3)
@@ -373,6 +371,9 @@
             else:
                 remote(src, rows.at[y, at(spot)], d_s, d_r.at[spot], (dst, tp)).start()
 
+    for copy in swap_w:
+        copy.start()
+
     for k in range(2):
         wts[k] = jnp.transpose(jnp.broadcast_to(rw[k : k + 1, :], (128, tok)))
         slot = jnp.transpose(jnp.broadcast_to(slot_rows[k].astype(F32), (128, tok)))
@@ -481,32 +482,38 @@
                     send_near()
 
     everything = pl.ds(0, slots)
-    for u in range(UNITS):
+    def pass_on(h, u):
+        for d in range(2):
+            hop_in(h, d, u).wait_recv()
+            hop(h + 1, d, u).start()
+
+    def enter(u):
         for k in range(2 * u * n_x, 2 * (u + 1) * n_x):
             spot = rows.at[y, at(k)]
             pltpu.make_async_copy(spot, spot, d_r.at[k]).wait()
         for d in range(2):
             hop(1, d, u).start()
 
+    def through(u):
+        for d in range(2):
+            hop_in(far, d, u).wait_recv()
+        finish(u)
+        first_sums(u)
+
+    for u in range(UNITS - 1):
+        enter(u)
+    pass_on(1, 0)
+    enter(UNITS - 1)
+
     for load in loads[1:4]:
         load.wait()
     for copy in swap_w:
         copy.wait_recv()
     accumulate(y, everything)
 
-    def pass_on(h, u):
-        for d in range(2):
-            hop_in(h, d, u).wait_recv()
-            hop(h + 1, d, u).start()
-
-    def through(u):
-        for d in range(2):
-            hop_in(far, d, u).wait_recv()
-        finish(u)
-        first_sums(u)
 
     for h in range(1, far - 1):
-        for u in range(UNITS):
+        for u in range(1 if h == 1 else 0, UNITS):
             pass_on(h, u)
         accumulate(chip(-h), everything)
         accumulate(chip(h), everything)

time: 88.4 us -> 88.4 us (level)
  no operation moved by 1% of the time
where the time goes in v6:
time: 88.4 us; the launch traced here: 88.2 us
  Pallas kernels  86.7 us (98%)
  local copies, waits for them, and re-layouts  1.47 us (2%)
    pallas_call x1, Pallas kernels, local(): pl.pallas_call(functools.partial(layer, n_sp, n_y), out_shape=jax.ShapeDt...  86.7 us

profile of v6, /device:TPU:1, one launch (start us, length us, event | category | flops | bytes accessed | tf_op | source)
XLA Modules:
  0.0 88.2 jit_solution(6240808441794996575)
XLA Ops:
  0.0 86.7 %shard_map.109 = bf16[256,128]{1,0:T(8,128)(2,1)} custom-call(bf16[64,256]{1,0:T(8,128)(2,1)} %bitcast.5, bf16[64,256]{1,0:T(8,128)(2,1)} %bitcast.6, bf16[31,64]{1,0:T(8,128)(2,1)} %taps_in.1, f32[1,64]{1,0:T(1,128)} %bitcast.9, bf16[64,2048]{1,0:T(8,128)(2,1)} %ow.1, bf16[256,2048]{1,0:T(8,128)(2,1)} %res.1, s32[2,256]{1,0:T(2,128)} %bitcast.7, ...), custom_call_target="tpu_custom_call" | custom-call | tf_op jit(solution)/shard_map/pallas_call | solution.py:623
  86.7 1.5 %copy.13 = bf16[256,128]{1,0:T(8,128)(2,1)} copy(bf16[256,128]{1,0:T(8,128)(2,1)} %shard_map.109) | data formatting | bytes 131072
